TPU v7x, 32 devices: a whole 2x2x4 slice. The times are simulated.
32 devices in a mesh: ep: 8 (over z, y), tp: 4 (over x, core).
Axes of the slice: x: 2, y: 2, z: 4, core: 2. Of those that a mesh axis runs over, the one named last changes fastest.
Arguments:
- queries: bfloat16 [8192, 1024], P('ep', 'tp'), may hold values from -6 to 6
- head_keys: bfloat16 [8192, 256], P('ep', 'tp'), may hold values from -6 to 6
- head_values: bfloat16 [8192, 256], P('ep', 'tp'), may hold values from -6 to 6
- sink_logits: float32 [16], P('tp'), may hold values from -2 to 5
- out_weight: bfloat16 [1024, 2048], P('tp'), may hold values from -1.5 to 1.5
- moe_input: bfloat16 [4096, 2048], P(('ep', 'tp')), may hold values from -6 to 6
- norm_gain: float32 [2048], replicated, may hold values from 0.1 to 1.9
- routes: int32 [4096, 4], P(('ep', 'tp')), may hold values from 0 to 7, all different within a row; in each aligned block of 128 rows (0 to 127, 128 to 255, ...) at most 128 rows name the same one
- route_weight: float32 [4096, 4], P(('ep', 'tp')), may hold values from 0.05 to 1
- gate_weight: bfloat16 [8, 2048, 512], P('ep'), may hold values from -2 to 2
- up_weight: bfloat16 [8, 2048, 512], P('ep'), may hold values from -2 to 2
- down_weight: bfloat16 [8, 512, 2048], P('ep'), may hold values from -0.25 to 0.25
Outputs:
- attention_out: bfloat16 [8192, 2048], P(('ep', 'tp'))
- routed_out: bfloat16 [4096, 2048], P(('ep', 'tp'))
Inputs may be any that keep to these rules, and one draw needn't show every extreme that they name: `routes`: within the rows of one device (aligned blocks of 128 rows), each expert is named by at most 128 rows, and in every draw some expert by exactly 128; a row names 4 different experts.
All inputs are finite; a program needn't handle non-finite values.
Results may differ from a plain program's by a relative error of at most 0.0078.
Values may be sent and summed in bfloat16 or wider, within the bound.
A program may use at most 128 MiB of HBM per device.

v0:
```python
import functools

import jax
import jax.numpy as jnp
from jax import lax
from jax.experimental import pallas as pl
from jax.experimental.pallas import tpu as pltpu
from jax.sharding import PartitionSpec as P

HEAD_DIM = 64
WINDOW = 128
SEQS = 1


EPSILON = 1e-05
NEGATIVE = -1e30


def passed_along(value, axis, steps):
    count = lax.axis_size(axis)
    first, last = (max(0, -steps), min(count, count - steps))
    return lax.ppermute(value, axis, [(source, source + steps) for source in range(first, last)])


def clamped_unit(gate_pre, up_pre):
    gate_cut = jnp.minimum(gate_pre, 7.0)
    up_cut = jnp.clip(up_pre, -7.0, 7.0)
    return gate_cut * jax.nn.sigmoid(1.702 * gate_cut) * (up_cut + 1.0)


def attend(queries, head_keys, head_values, sink_logits, out_weight):
    tok_rows = queries.shape[0]
    local_heads = sink_logits.shape[0]
    local_kv = head_keys.shape[1] // HEAD_DIM
    per_group = local_heads // local_kv
    block_count = tok_rows // WINDOW
    key_width = local_kv * HEAD_DIM
    kv_rows = jnp.concatenate([head_keys, head_values], axis=1)
    earlier = passed_along(kv_rows[tok_rows - WINDOW :], "ep", 1)
    extended = jnp.concatenate([earlier, kv_rows], axis=0)
    banded = jnp.concatenate(
        [
            extended[:tok_rows].reshape(block_count, WINDOW, 2 * key_width),
            kv_rows.reshape(block_count, WINDOW, 2 * key_width),
        ],
        axis=1,
    )
    band_keys = banded[:, :, :key_width].reshape(block_count, 2 * WINDOW, local_kv, HEAD_DIM)
    band_values = banded[:, :, key_width:].reshape(block_count, 2 * WINDOW, local_kv, HEAD_DIM)
    blocked = queries.reshape(block_count, WINDOW, local_kv, per_group, HEAD_DIM)
    scores = jnp.einsum(
        "nqkgd,nskd->nkgqs", blocked, band_keys, preferred_element_type=jnp.float32
    ) * HEAD_DIM ** (-0.5)
    offset = lax.axis_index("ep") * tok_rows
    seq_len = tok_rows * lax.axis_size("ep") // SEQS
    query_pos = offset + jnp.arange(tok_rows, dtype=jnp.int32).reshape(block_count, WINDOW)
    key_pos = (
        offset
        - WINDOW
        + (jnp.arange(block_count, dtype=jnp.int32) * WINDOW)[:, None]
        + jnp.arange(2 * WINDOW, dtype=jnp.int32)[None, :]
    )
    distance = query_pos[:, :, None] - key_pos[:, None, :]
    starts = query_pos // seq_len * seq_len
    valid = (distance >= 0) & (distance < WINDOW) & (key_pos[:, None, :] >= starts[:, :, None])
    scores = jnp.where(valid[:, None, None], scores, NEGATIVE)
    sinks = sink_logits.reshape(local_kv, per_group, 1, 1)
    maxima = jnp.maximum(jnp.max(scores, axis=-1, keepdims=True), sinks)
    powers = jnp.exp(scores - maxima)
    weights = (powers / (jnp.sum(powers, axis=-1, keepdims=True) + jnp.exp(sinks - maxima))).astype(
        jnp.bfloat16
    )
    heads_out = jnp.einsum(
        "nkgqs,nskd->nqkgd", weights, band_values, preferred_element_type=jnp.float32
    )
    heads_out = heads_out.astype(jnp.bfloat16).reshape(tok_rows, local_heads * HEAD_DIM)
    summed = lax.psum_scatter(
        jnp.dot(heads_out, out_weight, preferred_element_type=jnp.float32),
        "tp",
        scatter_dimension=0,
        tiled=True,
    )
    return summed.astype(jnp.bfloat16)


def experts_part(moe_input, norm_gain, routes, route_weight, gate_weight, up_weight, down_weight):
    tok_rows, model_width = moe_input.shape
    choice_count = routes.shape[1]
    targets = lax.axis_size("ep")
    capacity = 2 * choice_count * tok_rows // targets
    values32 = moe_input.astype(jnp.float32)
    scale = lax.rsqrt(jnp.mean(values32 * values32, axis=-1, keepdims=True) + EPSILON)
    normed = (values32 * scale * norm_gain).astype(jnp.bfloat16)
    if capacity >= tok_rows and targets % ROW == 0 and targets >= 2 * ROW:
        experts = jnp.arange(targets, dtype=jnp.int32)
        named = routes[:, None, :] == experts[None, :, None]
        shares = jnp.sum(jnp.where(named, route_weight[:, None, :], 0.0), axis=2).T
        return fused_experts(normed, shares, gate_weight[0], up_weight[0], down_weight[0])
    if capacity >= tok_rows:
        experts = jnp.arange(targets, dtype=jnp.int32)
        named = routes[:, :, None] == experts[None, None, :]
        shares = jnp.sum(jnp.where(named, route_weight[:, :, None], 0.0), axis=1)
        everyone = lax.all_gather(normed, "ep", axis=0, tiled=True)
        mine = lax.all_to_all(shares.T[:, None], "ep", split_axis=0, concat_axis=0, tiled=True)
        gate_pre = jnp.dot(everyone, gate_weight[0], preferred_element_type=jnp.float32)
        up_pre = jnp.dot(everyone, up_weight[0], preferred_element_type=jnp.float32)
        act = clamped_unit(gate_pre, up_pre).astype(jnp.bfloat16)
        result = jnp.dot(act, down_weight[0], preferred_element_type=jnp.float32)
        part = result.astype(jnp.bfloat16).astype(jnp.float32) * mine.reshape(-1, 1)
        return lax.psum_scatter(
            part.astype(jnp.bfloat16), "ep", scatter_dimension=0, tiled=True
        )
    flat_routes = routes.reshape(-1)
    onehot = (flat_routes[:, None] == jnp.arange(targets, dtype=jnp.int32)[None, :]).astype(
        jnp.int32
    )
    earlier_count = jnp.sum((jnp.cumsum(onehot, axis=0) - onehot) * onehot, axis=1)
    slot_index = flat_routes * capacity + earlier_count
    copies = jnp.repeat(normed, choice_count, axis=0)
    outgoing = jnp.zeros((targets * capacity, model_width), jnp.bfloat16).at[slot_index].set(copies)
    outgoing = outgoing.reshape(targets, capacity, model_width)
    arrived = lax.all_to_all(outgoing, "ep", split_axis=0, concat_axis=0, tiled=True)
    flat_rows = arrived.reshape(-1, model_width)
    gate_pre = jnp.dot(flat_rows, gate_weight[0], preferred_element_type=jnp.float32)
    up_pre = jnp.dot(flat_rows, up_weight[0], preferred_element_type=jnp.float32)
    act = clamped_unit(gate_pre, up_pre).astype(jnp.bfloat16)
    result = jnp.dot(act, down_weight[0], preferred_element_type=jnp.float32).astype(jnp.bfloat16)
    came_back = lax.all_to_all(
        result.reshape(arrived.shape), "ep", split_axis=0, concat_axis=0, tiled=True
    )
    picked = came_back.reshape(targets * capacity, model_width)[slot_index]
    weighted = (
        picked.astype(jnp.float32).reshape(tok_rows, choice_count, model_width)
        * route_weight[:, :, None]
    )
    return jnp.sum(weighted, axis=1).astype(jnp.bfloat16)


ROW = 2
PIECES = 2


def experts_kernel(
    count, rows_hbm, shares_hbm, gate_hbm, up_hbm, down_hbm, out_ref,
    gath, shares, gate_w, up_w, down_w, parts, from_row, onward, from_line,
    local_sem, share_send, share_recv, got, sent_up, sent_down, sent_row,
    row_send, row_recv, line_send, line_recv,
):
    lines = count // ROW
    me = lax.axis_index("ep")
    z, y = me // ROW, me % ROW
    tok_rows = out_ref.shape[0]
    piece = tok_rows // PIECES
    loads = [
        pltpu.make_async_copy(rows_hbm, gath.at[me], local_sem.at[0]),
        pltpu.make_async_copy(shares_hbm, shares.at[me], local_sem.at[1]),
        pltpu.make_async_copy(gate_hbm, gate_w, local_sem.at[2]),
        pltpu.make_async_copy(up_hbm, up_w, local_sem.at[3]),
        pltpu.make_async_copy(down_hbm, down_w, local_sem.at[4]),
    ]
    for load in loads:
        load.start()

    barrier = pltpu.get_barrier_semaphore()
    for step in range(1, count):
        other = lax.rem(me + step, count)
        pl.semaphore_signal(
            barrier, inc=1, device_id={"ep": other}, device_id_type=pl.DeviceIdType.MESH
        )
    pl.semaphore_wait(barrier, count - 1)

    def remote(source, target, send, recv, device):
        return pltpu.make_async_remote_copy(
            src_ref=source,
            dst_ref=target,
            send_sem=send,
            recv_sem=recv,
            device_id={"ep": device},
            device_id_type=pl.DeviceIdType.MESH,
        )

    def share_copy(slot, recv_slot, device):
        return remote(
            shares.at[slot], shares.at[slot], share_send.at[device], share_recv.at[recv_slot], device
        )

    def block_copy(block, h, sems, device):
        view = gath.at[block, pl.ds(h * piece, piece)]
        return remote(view, view, sems.at[block, h], got.at[block, h], device)

    across = z * ROW + (1 - y)
    above = jnp.minimum(z + 1, lines - 1) * ROW + y
    below = jnp.maximum(z - 1, 0) * ROW + y

    loads[0].wait()
    loads[1].wait()
    for h in range(PIECES):
        block_copy(me, h, sent_row, across).start()

        @pl.when(z < lines - 1)
        def _():
            block_copy(me, h, sent_up, above).start()

        @pl.when(z > 0)
        def _():
            block_copy(me, h, sent_down, below).start()

    for step in range(1, count):
        share_copy(me, me, lax.rem(me + step, count)).start()
    for step in range(1, count):
        source = lax.rem(me + step, count)
        remote(
            shares.at[source], shares.at[source], share_send.at[source],
            share_recv.at[source], source,
        ).wait_recv()
    loads[2].wait()
    loads[3].wait()
    loads[4].wait()

    square = (tok_rows, tok_rows)
    eye = lax.broadcasted_iota(jnp.int32, square, 0) == lax.broadcasted_iota(jnp.int32, square, 1)

    def visit(turn, carry):
        distance = turn // 4
        foreign = (turn // 2) % 2
        downward = turn % 2
        line = jnp.where(downward == 1, z + distance, z - distance)
        valid = (line >= 0) & (line < lines) & ((distance > 0) | (downward == 0))
        held = jnp.clip(line, 0, lines - 1) * ROW + jnp.where(foreign == 1, 1 - y, y)

        @pl.when(valid)
        def _():
            for h in range(PIECES):

                @pl.when(held != me)
                def _():
                    block_copy(held, h, sent_row, across).wait_recv()

                @pl.when((foreign == 0) & (distance > 0))
                def _():
                    block_copy(held, h, sent_row, across).start()

                    @pl.when((downward == 0) & (z < lines - 1))
                    def _():
                        block_copy(held, h, sent_up, above).start()

                    @pl.when((downward == 1) & (z > 0))
                    def _():
                        block_copy(held, h, sent_down, below).start()

            rows = gath[held]
            gate_pre = jnp.dot(rows, gate_w[...], preferred_element_type=jnp.float32)
            up_pre = jnp.dot(rows, up_w[...], preferred_element_type=jnp.float32)
            act = clamped_unit(gate_pre, up_pre).astype(jnp.bfloat16)
            share = shares[held, pl.ds(me, 1), :]
            column = jnp.sum(jnp.where(eye, share, 0.0), axis=1, keepdims=True)
            result = jnp.dot(act, down_w[...], preferred_element_type=jnp.float32)
            weighted = result.astype(jnp.bfloat16).astype(jnp.float32) * column
            parts[held] = weighted.astype(jnp.bfloat16)

        return carry

    lax.fori_loop(0, 4 * lines, visit, 0)

    def row_copy(line, h):
        return remote(
            parts.at[line * ROW + (1 - y), pl.ds(h * piece, piece)],
            from_row.at[line, pl.ds(h * piece, piece)],
            row_send.at[line, h],
            row_recv.at[line, h],
            across,
        )

    def line_copy(line, h, downward, device):
        return remote(
            onward.at[line, pl.ds(h * piece, piece)],
            from_line.at[downward, line, pl.ds(h * piece, piece)],
            line_send.at[line, h],
            line_recv.at[downward, line, h],
            device,
        )

    def far_first(turn):
        distance = lines - 1 - turn // 2
        downward = turn % 2
        line = jnp.where(downward == 1, z - distance, z + distance)
        valid = (line >= 0) & (line < lines)
        return distance, downward, valid, jnp.clip(line, 0, lines - 1)

    def send_across(turn, carry):
        distance, downward, valid, line = far_first(turn)

        @pl.when(valid & ((distance > 0) | (downward == 0)))
        def _():
            for h in range(PIECES):
                row_copy(line, h).start()

        return carry

    lax.fori_loop(0, 2 * lines, send_across, 0)

    def pass_on(turn, carry):
        distance, downward, valid, line = far_first(turn)

        @pl.when(valid)
        def _():
            for h in range(PIECES):
                span = pl.ds(h * piece, piece)
                row_copy(line, h).wait_recv()
                base = parts[line * ROW + y, span].astype(jnp.float32) + from_row[
                    line, span
                ].astype(jnp.float32)

                @pl.when(downward == 0)
                def _():
                    @pl.when(z > 0)
                    def _():
                        line_copy(line, h, 0, above).wait_recv()
                        onward[line, span] = (
                            base + from_line[0, line, span].astype(jnp.float32)
                        ).astype(jnp.bfloat16)

                    @pl.when(z == 0)
                    def _():
                        onward[line, span] = base.astype(jnp.bfloat16)

                    line_copy(line, h, 0, above).start()

                @pl.when(downward == 1)
                def _():
                    @pl.when(z < lines - 1)
                    def _():
                        line_copy(line, h, 1, below).wait_recv()
                        onward[line, span] = (
                            base + from_line[1, line, span].astype(jnp.float32)
                        ).astype(jnp.bfloat16)

                    @pl.when(z == lines - 1)
                    def _():
                        onward[line, span] = base.astype(jnp.bfloat16)

                    line_copy(line, h, 1, below).start()

        return carry

    lax.fori_loop(0, 2 * (lines - 1), pass_on, 0)

    for h in range(PIECES):
        span = pl.ds(h * piece, piece)
        place = slice(h * piece, (h + 1) * piece)
        row_copy(z, h).wait_recv()
        base = parts[me, span].astype(jnp.float32) + from_row[z, span].astype(jnp.float32)

        @pl.when(z > 0)
        def _():
            line_copy(z, h, 0, above).wait_recv()

        @pl.when(z < lines - 1)
        def _():
            line_copy(z, h, 1, below).wait_recv()

        @pl.when(z == 0)
        def _():
            total = base + from_line[1, z, span].astype(jnp.float32)
            out_ref[place] = total.astype(jnp.bfloat16)

        @pl.when(z == lines - 1)
        def _():
            total = base + from_line[0, z, span].astype(jnp.float32)
            out_ref[place] = total.astype(jnp.bfloat16)

        @pl.when((z > 0) & (z < lines - 1))
        def _():
            total = base + (
                from_line[0, z, span].astype(jnp.float32)
                + from_line[1, z, span].astype(jnp.float32)
            )
            out_ref[place] = total.astype(jnp.bfloat16)

    for step in range(1, count):
        share_copy(me, me, lax.rem(me + step, count)).wait_send()

    def finish(line, carry):
        held = line * ROW + y
        for h in range(PIECES):
            block_copy(held, h, sent_row, across).wait_send()
            row_copy(line, h).wait_send()

            @pl.when((line <= z) & (z < lines - 1))
            def _():
                block_copy(held, h, sent_up, above).wait_send()

            @pl.when((line >= z) & (z > 0))
            def _():
                block_copy(held, h, sent_down, below).wait_send()

            @pl.when(line != z)
            def _():
                line_copy(line, h, 0, above).wait_send()

        return carry

    lax.fori_loop(0, lines, finish, 0)


def fused_experts(normed, shares, gate_weight, up_weight, down_weight):
    count = lax.axis_size("ep")
    lines = count // ROW
    tok_rows, width = normed.shape
    hidden = gate_weight.shape[1]
    block = (tok_rows, width)
    sem = pltpu.SemaphoreType.DMA
    flops = 6 * count * tok_rows * width * hidden
    return pl.pallas_call(
        functools.partial(experts_kernel, count),
        out_shape=jax.ShapeDtypeStruct(block, jnp.bfloat16),
        in_specs=[pl.BlockSpec(memory_space=pl.ANY)] * 5,
        out_specs=pl.BlockSpec(memory_space=pltpu.VMEM),
        scratch_shapes=[
            pltpu.VMEM((count,) + block, jnp.bfloat16),
            pltpu.VMEM((count, count, tok_rows), jnp.float32),
            pltpu.VMEM((width, hidden), jnp.bfloat16),
            pltpu.VMEM((width, hidden), jnp.bfloat16),
            pltpu.VMEM((hidden, width), jnp.bfloat16),
            pltpu.VMEM((count,) + block, jnp.bfloat16),
            pltpu.VMEM((lines,) + block, jnp.bfloat16),
            pltpu.VMEM((lines,) + block, jnp.bfloat16),
            pltpu.VMEM((2, lines) + block, jnp.bfloat16),
            sem((5,)),
            sem((count,)),
            sem((count,)),
            sem((count, PIECES)),
            sem((count, PIECES)),
            sem((count, PIECES)),
            sem((count, PIECES)),
            sem((lines, PIECES)),
            sem((lines, PIECES)),
            sem((lines, PIECES)),
            sem((2, lines, PIECES)),
        ],
        compiler_params=pltpu.CompilerParams(
            collective_id=0, has_side_effects=True, vmem_limit_bytes=44 * 1024 * 1024
        ),
        cost_estimate=pl.CostEstimate(
            flops=10 * flops, bytes_accessed=count * tok_rows * width * 8, transcendentals=0
        ),
    )(normed, shares, gate_weight, up_weight, down_weight)


def on_device(
    queries,
    head_keys,
    head_values,
    sink_logits,
    out_weight,
    moe_input,
    norm_gain,
    routes,
    route_weight,
    gate_weight,
    up_weight,
    down_weight,
):
    attention_out = attend(queries, head_keys, head_values, sink_logits, out_weight)
    routed_out = experts_part(
        moe_input, norm_gain, routes, route_weight, gate_weight, up_weight, down_weight
    )
    return (attention_out, routed_out)


def solution(mesh):
    placed = (
        P("ep", "tp"),
        P("ep", "tp"),
        P("ep", "tp"),
        P("tp"),
        P("tp", None),
        P(("ep", "tp"), None),
        P(),
        P(("ep", "tp"), None),
        P(("ep", "tp"), None),
        P("ep", None, None),
        P("ep", None, None),
        P("ep", None, None),
    )
    return jax.shard_map(
        on_device,
        mesh=mesh,
        in_specs=placed,
        out_specs=(P(("ep", "tp"), None), P(("ep", "tp"), None)),
        check_vma=False,
    )
```

profile of v0, /device:TPU:0, one launch (start us, length us, event | category | flops | bytes accessed | tf_op | source)
XLA Modules:
  0.0 149.6 jit_solution(12019236724930373127)
XLA Ops:
  7.2 0.0 copy-start
  7.2 0.0 reduce-scatter.2.cloned.1.call-start
  7.2 1.1 copy.28
  8.4 1.1 copy.29
  9.5 0.1 fusion.27
  9.6 4.9 %collective-permute-start = (bf16[128,128]{1,0:T(8,128)(2,1)S(1)}, bf16[128,128]{1,0:T(8,128)(2,1)S(1)}, u32[]{:S(2)}, u32[]{:S(2)}) collective-permute-start(bf16[128,128]{1,0:T(8,128)(2,1)S(1)} %fusion.27), channel_id=1, source_target_pairs={{0,4},{4,8},{8,12},{12,16},{16,20},{20,24},{24,28},{1,5},{5,9},{9,... | collective-permute-start | bytes 98312 | tf_op jit(solution)/shard_map/ppermute | solution.py:22
  14.5 0.1 iota_add_fusion
  14.6 0.5 fusion.17
  15.1 2.0 %reshape.148 = bf16[8,128,4,64]{3,2,1,0:T(4,128)(2,1)S(1)} reshape(bf16[1024,256]{1,0:T(8,128)(2,1)} %param.12) | data formatting | bytes 1048576 | tf_op jit(solution)/shard_map/reshape.2
  17.1 0.2 pad_maximum_fusion.1
  17.3 0.2 copy.30
  17.5 0.2 copy.31
  17.7 0.9 fusion.1
  18.6 0.1 broadcast_maximum_fusion
  18.7 1.0 fusion
  19.7 0.1 exponential_add_fusion
  19.8 1.2 fusion.8
  21.0 0.3 copy.35
  21.4 4.5 %fusion.18 = f32[1024,2048]{1,0:T(8,128)} fusion(bf16[256,2048]{1,0:T(8,128)(2,1)S(1)} %copy-done, bf16[32,8,8,128]{3,2,1,0:T(8,128)(2,1)S(1)} %bitcast.58), kind=kOutput, calls=%fused_computation.21 | convolution fusion | flops 1073741824 | bytes 9961472 | tf_op jit(solution)/shard_map/dot_general | solution.py:78
  25.9 0.0 reduce-scatter.2.cloned.1.call-update
  25.9 0.6 copy-done.7
  26.6 0.0 copy-done.8
  26.6 0.4 copy-done.4
  27.0 0.2 fusion.11
  27.2 0.2 fusion.13.rows_hbm
  27.4 1.6 %copy-done.1 = bf16[1,2048,512]{2,1,0:T(8,128)(2,1)S(1)} copy-done((bf16[1,2048,512]{2,1,0:T(8,128)(2,1)S(1)}, bf16[1,2048,512]{2,1,0:T(8,128)(2,1)}, u32[]{:S(2)}) %copy-start.1) | copy-done | bytes 2097176
  29.0 1.6 %copy-done.2 = bf16[1,2048,512]{2,1,0:T(8,128)(2,1)S(1)} copy-done((bf16[1,2048,512]{2,1,0:T(8,128)(2,1)S(1)}, bf16[1,2048,512]{2,1,0:T(8,128)(2,1)}, u32[]{:S(2)}) %copy-start.2) | copy-done | bytes 2097176
  30.6 1.6 %copy-done.3 = bf16[1,512,2048]{2,1,0:T(8,128)(2,1)S(1)} copy-done((bf16[1,512,2048]{2,1,0:T(8,128)(2,1)S(1)}, bf16[1,512,2048]{2,1,0:T(8,128)(2,1)}, u32[]{:S(2)}) %copy-start.3) | copy-done | bytes 2097176
  32.2 107.0 %shard_map.131 = bf16[128,2048]{1,0:T(8,128)(2,1)S(1)} custom-call(bf16[128,2048]{1,0:T(8,128)(2,1)S(1)} %fusion.13.rows_hbm, f32[8,128]{1,0:T(8,128)S(1)} %bitcast.54, bf16[2048,512]{1,0:T(8,128)(2,1)S(1)} %bitcast.55, bf16[2048,512]{1,0:T(8,128)(2,1)S(1)} %bitcast.56, bf16[512,2048]{1,0:T(8,128)(2,1)S(1)} %bitcast.57), custom_call_target="tpu_custom_call" | custom-call | flops 64424509440 | bytes 16777216 | tf_op jit(solution)/shard_map/pallas_call | solution.py:414
  139.2 0.0 reduce-scatter.2.cloned.1.call-done
  139.2 2.7 %convert_element_type.25 = bf16[256,2048]{1,0:T(8,128)(2,1)} convert(f32[256,2048]{1,0:T(8,128)} %reduce-scatter.2.cloned.1.call-done) | non-fusion elementwise | flops 524288 | bytes 3145728 | tf_op jit(solution)/shard_map/convert_element_type | solution.py:83
  141.9 0.8 copy.51
  (16 shorter events, 0.1 us)
Async XLA Ops:
  7.2 14.2 %copy-start = (bf16[256,2048]{1,0:T(8,128)(2,1)S(1)}, bf16[256,2048]{1,0:T(8,128)(2,1)}, u32[]{:S(2)}) copy-start(bf16[256,2048]{1,0:T(8,128)(2,1)} %param.16) | copy-start | bytes 3145732
  7.2 132.0 %reduce-scatter.2.cloned.1.call-start = ((), (), s32[]{:S(2)}) async-start(), calls=%async_computation.1 | async-start | bytes 10485760 | tf_op jit(solution)/shard_map/reduce_scatter | solution.py:77
  9.6 7.6 %collective-permute-start = (bf16[128,128]{1,0:T(8,128)(2,1)S(1)}, bf16[128,128]{1,0:T(8,128)(2,1)S(1)}, u32[]{:S(2)}, u32[]{:S(2)}) collective-permute-start(bf16[128,128]{1,0:T(8,128)(2,1)S(1)} %fusion.27), channel_id=1, source_target_pairs={{0,4},{4,8},{8,12},{12,16},{16,20},{20,24},{24,28},{1,5},{5,9},{9,... | collective-permute-start | bytes 98312 | tf_op jit(solution)/shard_map/ppermute | solution.py:22
  17.1 1.5 %copy-start.6 = (f32[4]{0:T(128)S(1)}, f32[4]{0:T(128)}, u32[]{:S(2)}) copy-start(f32[4]{0:T(128)} %param.15) | copy-start | bytes 52
  25.9 0.7 copy-start.7
  25.9 0.7 copy-start.8
  25.9 1.1 copy-start.4
  25.9 1.3 copy-start.5
  27.4 1.6 %copy-start.1 = (bf16[1,2048,512]{2,1,0:T(8,128)(2,1)S(1)}, bf16[1,2048,512]{2,1,0:T(8,128)(2,1)}, u32[]{:S(2)}) copy-start(bf16[1,2048,512]{2,1,0:T(8,128)(2,1)} %param.21) | copy-start | bytes 6291460
  29.0 1.6 %copy-start.2 = (bf16[1,2048,512]{2,1,0:T(8,128)(2,1)S(1)}, bf16[1,2048,512]{2,1,0:T(8,128)(2,1)}, u32[]{:S(2)}) copy-start(bf16[1,2048,512]{2,1,0:T(8,128)(2,1)} %param.22) | copy-start | bytes 6291460
  30.6 1.6 %copy-start.3 = (bf16[1,512,2048]{2,1,0:T(8,128)(2,1)S(1)}, bf16[1,512,2048]{2,1,0:T(8,128)(2,1)}, u32[]{:S(2)}) copy-start(bf16[1,512,2048]{2,1,0:T(8,128)(2,1)} %param.23) | copy-start | bytes 6291460
Sparse Core Ops, SparseCore 0:
  26.1 72.3 reduce-scatter.1
where the time goes:
time: 150 us
  Pallas kernels  107 us (71%)
  between operations  14.2 us (9%)
  local copies, waits for them, and re-layouts  11.6 us (8%)
  matrix products  6.63 us (4%)
  other arithmetic  5.15 us (3%)
  starting transfers between devices  4.94 us (3%)
    pallas_call x1, Pallas kernels, fused_experts(): pl.pallas_call(functools.partial(experts_kernel, count), out_shape=jax.Sh...  107 us
    unnamed x21, local copies, waits for them, and re-layouts  8.84 us
    ppermute x1, starting transfers between devices, passed_along(): lax.ppermute(value, axis, [(source, source + steps) for source in range(f...  4.9 us
    dot_general x1, matrix products, attend(): jnp.dot(heads_out, out_weight, preferred_element_type=jnp.float32)  4.51 us
  transfers between devices with their start and end apart: 2, of which 0 were waited for; matrix products, arithmetic and copies ran while one was open for 2% of the time, Pallas kernels for 72%

commit v1 on v0

v1 whole, which is shorter than its diff:
```python
import functools

import jax
import jax.numpy as jnp
from jax import lax
from jax.experimental import pallas as pl
from jax.experimental.pallas import tpu as pltpu
from jax.sharding import PartitionSpec as P

HEAD_DIM = 64
WINDOW = 128
SEQS = 1


EPSILON = 1e-05
NEGATIVE = -1e30


def passed_along(value, axis, steps):
    count = lax.axis_size(axis)
    first, last = (max(0, -steps), min(count, count - steps))
    return lax.ppermute(value, axis, [(source, source + steps) for source in range(first, last)])


def clamped_unit(gate_pre, up_pre):
    gate_cut = jnp.minimum(gate_pre, 7.0)
    up_cut = jnp.clip(up_pre, -7.0, 7.0)
    return gate_cut * jax.nn.sigmoid(1.702 * gate_cut) * (up_cut + 1.0)


def attend(queries, head_keys, head_values, sink_logits, out_weight):
    tok_rows = queries.shape[0]
    local_heads = sink_logits.shape[0]
    local_kv = head_keys.shape[1] // HEAD_DIM
    per_group = local_heads // local_kv
    block_count = tok_rows // WINDOW
    key_width = local_kv * HEAD_DIM
    kv_rows = jnp.concatenate([head_keys, head_values], axis=1)
    earlier = passed_along(kv_rows[tok_rows - WINDOW :], "ep", 1)
    extended = jnp.concatenate([earlier, kv_rows], axis=0)
    banded = jnp.concatenate(
        [
            extended[:tok_rows].reshape(block_count, WINDOW, 2 * key_width),
            kv_rows.reshape(block_count, WINDOW, 2 * key_width),
        ],
        axis=1,
    )
    band_keys = banded[:, :, :key_width].reshape(block_count, 2 * WINDOW, local_kv, HEAD_DIM)
    band_values = banded[:, :, key_width:].reshape(block_count, 2 * WINDOW, local_kv, HEAD_DIM)
    blocked = queries.reshape(block_count, WINDOW, local_kv, per_group, HEAD_DIM)
    scores = jnp.einsum(
        "nqkgd,nskd->nkgqs", blocked, band_keys, preferred_element_type=jnp.float32
    ) * HEAD_DIM ** (-0.5)
    offset = lax.axis_index("ep") * tok_rows
    seq_len = tok_rows * lax.axis_size("ep") // SEQS
    query_pos = offset + jnp.arange(tok_rows, dtype=jnp.int32).reshape(block_count, WINDOW)
    key_pos = (
        offset
        - WINDOW
        + (jnp.arange(block_count, dtype=jnp.int32) * WINDOW)[:, None]
        + jnp.arange(2 * WINDOW, dtype=jnp.int32)[None, :]
    )
    distance = query_pos[:, :, None] - key_pos[:, None, :]
    starts = query_pos // seq_len * seq_len
    valid = (distance >= 0) & (distance < WINDOW) & (key_pos[:, None, :] >= starts[:, :, None])
    scores = jnp.where(valid[:, None, None], scores, NEGATIVE)
    sinks = sink_logits.reshape(local_kv, per_group, 1, 1)
    maxima = jnp.maximum(jnp.max(scores, axis=-1, keepdims=True), sinks)
    powers = jnp.exp(scores - maxima)
    weights = (powers / (jnp.sum(powers, axis=-1, keepdims=True) + jnp.exp(sinks - maxima))).astype(
        jnp.bfloat16
    )
    heads_out = jnp.einsum(
        "nkgqs,nskd->nqkgd", weights, band_values, preferred_element_type=jnp.float32
    )
    heads_out = heads_out.astype(jnp.bfloat16).reshape(tok_rows, local_heads * HEAD_DIM)
    summed = lax.psum_scatter(
        jnp.dot(heads_out, out_weight, preferred_element_type=jnp.float32),
        "tp",
        scatter_dimension=0,
        tiled=True,
    )
    return summed.astype(jnp.bfloat16)


def experts_part(moe_input, norm_gain, routes, route_weight, gate_weight, up_weight, down_weight):
    tok_rows, model_width = moe_input.shape
    choice_count = routes.shape[1]
    targets = lax.axis_size("ep")
    capacity = 2 * choice_count * tok_rows // targets
    values32 = moe_input.astype(jnp.float32)
    scale = lax.rsqrt(jnp.mean(values32 * values32, axis=-1, keepdims=True) + EPSILON)
    normed = (values32 * scale * norm_gain).astype(jnp.bfloat16)
    if capacity >= tok_rows:
        experts = jnp.arange(targets, dtype=jnp.int32)
        named = routes[:, :, None] == experts[None, None, :]
        shares = jnp.sum(jnp.where(named, route_weight[:, :, None], 0.0), axis=1)
        everyone = lax.all_gather(normed, "ep", axis=0, tiled=True)
        mine = lax.all_to_all(shares.T[:, None], "ep", split_axis=0, concat_axis=0, tiled=True)
        gate_pre = jnp.dot(everyone, gate_weight[0], preferred_element_type=jnp.float32)
        up_pre = jnp.dot(everyone, up_weight[0], preferred_element_type=jnp.float32)
        act = clamped_unit(gate_pre, up_pre).astype(jnp.bfloat16)
        result = jnp.dot(act, down_weight[0], preferred_element_type=jnp.float32)
        part = result.astype(jnp.bfloat16).astype(jnp.float32) * mine.reshape(-1, 1)
        return lax.psum_scatter(
            part.astype(jnp.bfloat16), "ep", scatter_dimension=0, tiled=True
        )
    flat_routes = routes.reshape(-1)
    onehot = (flat_routes[:, None] == jnp.arange(targets, dtype=jnp.int32)[None, :]).astype(
        jnp.int32
    )
    earlier_count = jnp.sum((jnp.cumsum(onehot, axis=0) - onehot) * onehot, axis=1)
    slot_index = flat_routes * capacity + earlier_count
    copies = jnp.repeat(normed, choice_count, axis=0)
    outgoing = jnp.zeros((targets * capacity, model_width), jnp.bfloat16).at[slot_index].set(copies)
    outgoing = outgoing.reshape(targets, capacity, model_width)
    arrived = lax.all_to_all(outgoing, "ep", split_axis=0, concat_axis=0, tiled=True)
    flat_rows = arrived.reshape(-1, model_width)
    gate_pre = jnp.dot(flat_rows, gate_weight[0], preferred_element_type=jnp.float32)
    up_pre = jnp.dot(flat_rows, up_weight[0], preferred_element_type=jnp.float32)
    act = clamped_unit(gate_pre, up_pre).astype(jnp.bfloat16)
    result = jnp.dot(act, down_weight[0], preferred_element_type=jnp.float32).astype(jnp.bfloat16)
    came_back = lax.all_to_all(
        result.reshape(arrived.shape), "ep", split_axis=0, concat_axis=0, tiled=True
    )
    picked = came_back.reshape(targets * capacity, model_width)[slot_index]
    weighted = (
        picked.astype(jnp.float32).reshape(tok_rows, choice_count, model_width)
        * route_weight[:, :, None]
    )
    return jnp.sum(weighted, axis=1).astype(jnp.bfloat16)


ROW = 2
CORES = 2
TP = 4
PIECES = 4
CHUNKS = 4
SLABS = 8
LAG = 2


def fused_kernel(
    lines, width,
    rows_hbm, shares_hbm, gate_hbm, up_hbm, down_hbm, q_hbm, kv_hbm, sinks_hbm, proj_hbm,
    routed_ref, attn_ref,
    gath, shares, wgu, wd, act, onward, from_line,
    qs, ext, sinks, wo, keep, mate_out, mate_in, x_out, x_in,
    local_sem, share_send, share_recv, halo_sem,
    up_send, down_send, tok_recv,
    y_send, y_recv, x_send, x_recv, m_send, m_recv,
    line_send, line_recv, pair_send, pair_recv, cross_send, cross_recv,
):
    ep, tp = lax.axis_index("ep"), lax.axis_index("tp")
    z, y, x, c = ep // ROW, ep % ROW, tp // CORES, tp % CORES
    tok_rows, model_width = routed_ref.shape
    hidden = gate_hbm.shape[1]
    piece = tok_rows // PIECES
    chunk = model_width // CHUNKS
    last = lines - 1

    def at(zz, yy, xx, cc):
        return {"ep": zz * ROW + yy, "tp": xx * CORES + cc}

    def remote(source, target, send, recv, device):
        return pltpu.make_async_remote_copy(
            src_ref=source, dst_ref=target, send_sem=send, recv_sem=recv,
            device_id=device, device_id_type=pl.DeviceIdType.MESH,
        )

    above = at(jnp.minimum(z + 1, last), y, x, c)
    below = at(jnp.maximum(z - 1, 0), y, x, c)
    over_y, over_x, mate = at(z, 1 - y, x, c), at(z, y, 1 - x, c), at(z, y, x, 1 - c)

    own_kv = ext.at[pl.ds(WINDOW, q_hbm.shape[0])]
    loads = [
        pltpu.make_async_copy(source, target, local_sem.at[i])
        for i, (source, target) in enumerate([
            (kv_hbm, own_kv),
            (rows_hbm, gath.at[z]),
            (shares_hbm, shares.at[z]),
            (gate_hbm, wgu.at[0, :, pl.ds(0, hidden)]),
            (up_hbm, wgu.at[0, :, pl.ds(hidden, hidden)]),
            (down_hbm, wd.at[pl.ds(0, hidden)]),
            (q_hbm, qs),
            (sinks_hbm, sinks),
            (proj_hbm, wo),
        ])
    ]
    for load in loads:
        load.start()

    ahead = ep + 1 < lines * ROW
    behind = ep > 0
    skew = jnp.where(y == 1, z < last, z > 0)
    skew_ep = jnp.where(y == 1, jnp.minimum(ep + 1, lines * ROW - 1), jnp.maximum(ep - 1, 0))
    barrier = pltpu.get_barrier_semaphore()

    def greet(device):
        pl.semaphore_signal(barrier, inc=1, device_id=device, device_id_type=pl.DeviceIdType.MESH)

    for step in range(1, lines):
        greet(at(lax.rem(z + step, lines), y, x, c))
    greet(over_y)
    greet(over_x)
    greet(mate)

    @pl.when(skew)
    def _():
        greet({"ep": skew_ep, "tp": tp})

    pl.semaphore_wait(barrier, last + 3 + jnp.where(skew, 1, 0))

    halo = remote(
        ext.at[pl.ds(q_hbm.shape[0], WINDOW)], ext.at[pl.ds(0, WINDOW)], halo_sem.at[0],
        halo_sem.at[1], {"ep": jnp.minimum(ep + 1, lines * ROW - 1), "tp": tp},
    )

    def share_copy(slot, recv_slot, device):
        return remote(
            shares.at[slot], shares.at[slot], share_send.at[recv_slot], share_recv.at[slot], device
        )

    def tok_copy(block, part, sems, device):
        view = gath.at[block, pl.ds(part * piece, piece)]
        return remote(view, view, sems.at[block, part], tok_recv.at[block, part], device)

    quarter = wgu.shape[1] // TP
    slab = quarter // SLABS

    def gu_view(expert, q, p):
        return wgu.at[expert, pl.ds(q * quarter + p * slab, slab)]

    def d_view(expert, q, p):
        return wd.at[
            pl.ds(expert * hidden + q * (hidden // TP), hidden // TP), pl.ds(p * chunk, chunk)
        ]

    def weight_copies(view, base):
        def over_link(p):
            return remote(
                view(0, tp, p), view(1, tp, p), y_send.at[base + p], y_recv.at[base + p], over_y
            )

        def to_plane(p):
            return remote(
                view(1, tp, p), view(1, tp, p), x_send.at[base + p], x_recv.at[base + p], over_x
            )

        def to_mate(p, second):
            q = jnp.where(second == 1, (1 - x) * CORES + c, tp) if second else tp
            return remote(
                view(1, q, p), view(1, q, p), m_send.at[second, base + p],
                m_recv.at[second, base + p], mate,
            )

        return over_link, to_plane, to_mate

    gu_over, gu_plane, gu_mate = weight_copies(gu_view, 0)
    d_over, d_plane, d_mate = weight_copies(d_view, SLABS)

    loads[0].wait()

    @pl.when(ahead)
    def _():
        halo.start()

    loads[1].wait()
    loads[2].wait()
    for step in range(1, lines):
        other = lax.rem(z + step, lines)
        share_copy(z, other, at(other, y, x, c)).start()

    def own_tokens(first, count, upward):
        for part in range(first, first + count):
            if upward:
                tok_copy(z, part, up_send, above).start()
            else:
                tok_copy(z, part, down_send, below).start()

    half = PIECES // 2

    @pl.when(z < last)
    def _():
        own_tokens(0, half, True)

    @pl.when(z == 0)
    def _():
        own_tokens(half, half, True)

    @pl.when(z > 0)
    def _():
        own_tokens(0, half, False)

    @pl.when(z == last)
    def _():
        own_tokens(half, half, False)

    loads[3].wait()
    loads[4].wait()

    def launch_gu(p, carry):
        gu_over(p).start()
        return carry

    lax.fori_loop(0, SLABS, launch_gu, 0)
    loads[5].wait()

    def launch_d(p, carry):
        d_over(p).start()
        return carry

    lax.fori_loop(0, CHUNKS, launch_d, 0)

    @pl.when(z == 0)
    def _():
        from_line[0] = jnp.zeros_like(from_line[0])

    @pl.when(z == last)
    def _():
        from_line[1] = jnp.zeros_like(from_line[1])

    loads[6].wait()
    loads[7].wait()
    loads[8].wait()

    @pl.when(behind)
    def _():
        halo.wait_recv()

    @pl.when(ep == 0)
    def _():
        ext[pl.ds(0, WINDOW)] = jnp.zeros((WINDOW, ext.shape[1]), ext.dtype)

    def arrival(i, reach):
        s = i // half
        far = s < reach
        distance = jnp.where(far, s + 1, 2 * reach - s)
        part = jnp.where(far, 0, half) + i % half
        return distance, part

    def pump_tokens(i):
        for upward in (True, False):
            reach = z if upward else last - z
            distance, part = arrival(i, reach)
            block = jnp.clip(z - distance if upward else z + distance, 0, last)

            @pl.when(i < PIECES * reach)
            def _():
                tok_copy(block, part, up_send, above).wait_recv()

            @pl.when((i < PIECES * reach) & (reach < last))
            def _():
                if upward:
                    tok_copy(block, part, up_send, above).start()
                else:
                    tok_copy(block, part, down_send, below).start()

            @pl.when((i == PIECES * reach - 1) & (reach < last))
            def _():
                own_tokens(half, half, upward)

    per_group = sinks.shape[0]
    band = 2 * WINDOW
    quarter_rows = attn_ref.shape[0]
    blocks_each = quarter_rows // WINDOW
    kv_width = ext.shape[1] // 2

    def pair_copy(owner_x):
        return remote(
            mate_out.at[owner_x], mate_in.at[owner_x], pair_send.at[owner_x],
            pair_recv.at[owner_x], mate,
        )

    def attend_block(n):
        q_rows = qs[pl.ds(n * WINDOW, WINDOW)] * jnp.bfloat16(HEAD_DIM ** (-0.5))
        held = ext[pl.ds(n * WINDOW, band)]
        keys = jnp.concatenate([held[:, :kv_width]] * 2, axis=1)
        values = jnp.concatenate([held[:, kv_width:]] * 2, axis=1)
        q_head = lax.broadcasted_iota(jnp.int32, q_rows.shape, 1) // HEAD_DIM
        stacked = jnp.concatenate(
            [jnp.where(q_head == h, q_rows, jnp.zeros_like(q_rows)) for h in range(per_group)],
            axis=0,
        )
        scores = lax.dot_general(
            stacked, keys, (((1,), (1,)), ((), ())), preferred_element_type=jnp.float32
        )
        begins = lax.rem(ep * (qs.shape[0] // WINDOW) + n, lines * ROW * (qs.shape[0] // WINDOW) // SEQS) == 0
        row = lax.broadcasted_iota(jnp.int32, (WINDOW, band), 0)
        col = lax.broadcasted_iota(jnp.int32, (WINDOW, band), 1)
        valid = (col > row) & (col <= row + WINDOW) & (col >= jnp.where(begins, WINDOW, 0))
        weights = []
        for h in range(per_group):
            score = jnp.where(valid, scores[h * WINDOW : (h + 1) * WINDOW], NEGATIVE)
            sink = sinks[h : h + 1, 0:1]
            top = jnp.maximum(jnp.max(score, axis=1, keepdims=True), sink)
            powers = jnp.exp(score - top)
            total = jnp.sum(powers, axis=1, keepdims=True) + jnp.exp(sink - top)
            weights.append((powers * (1.0 / total)).astype(jnp.bfloat16))
        v_head = lax.broadcasted_iota(jnp.int32, values.shape, 1) // HEAD_DIM
        spread = jnp.concatenate(
            [jnp.where(v_head == h, values, jnp.zeros_like(values)) for h in range(per_group)],
            axis=0,
        )
        heads = jnp.dot(
            jnp.concatenate(weights, axis=1), spread, preferred_element_type=jnp.float32
        ).astype(jnp.bfloat16)
        owner = n // blocks_each
        owner_x, owner_c = owner // CORES, owner % CORES
        place = pl.ds((n % blocks_each) * WINDOW, WINDOW)
        share = jnp.dot(heads, wo[...], preferred_element_type=jnp.float32)

        @pl.when(owner_c == c)
        def _():
            keep[owner_x, place] = share

        @pl.when(owner_c != c)
        def _():
            mate_out[owner_x, place] = share.astype(jnp.bfloat16)

    def slot(i, carry):
        gu_over(i).wait_recv()
        gu_plane(i).start()
        gu_mate(i, 0).start()
        pump_tokens(i)

        @pl.when(i >= LAG)
        def _():
            gu_plane(i - LAG).wait_recv()
            gu_mate(i - LAG, 1).start()

        attend_block(i)
        return carry

    lax.fori_loop(0, SLABS, slot, 0)
    for owner_x in range(TP // CORES):
        pair_copy(owner_x).start()
    for p in range(SLABS - LAG, SLABS):
        gu_plane(p).wait_recv()
        gu_mate(p, 1).start()
    for step in range(1, lines):
        source = lax.rem(z + step, lines)
        share_copy(source, source, at(source, y, x, c)).wait_recv()

    def gather_gu(p, carry):
        gu_mate(p, 0).wait_recv()
        gu_mate(p, 1).wait_recv()
        return carry

    lax.fori_loop(0, SLABS, gather_gu, 0)

    square = (tok_rows, tok_rows)
    eye = lax.broadcasted_iota(jnp.int32, square, 0) == lax.broadcasted_iota(jnp.int32, square, 1)

    def activate(block):
        def one(expert, carry):
            pre = jnp.dot(gath[block], wgu[expert], preferred_element_type=jnp.float32)
            unit = clamped_unit(pre[:, :hidden], pre[:, hidden:])
            named = z * ROW + jnp.where(expert == 1, 1 - y, y)
            column = jnp.sum(
                jnp.where(eye, shares[block, pl.ds(named, 1), :], 0.0), axis=1, keepdims=True
            )
            act[expert] = (unit * column).astype(jnp.bfloat16)
            return carry

        lax.fori_loop(0, ROW, one, 0)

    def partial(cols):
        both = jnp.concatenate([act[0], act[1]], axis=1)
        return jnp.dot(both, wd[:, cols], preferred_element_type=jnp.float32)

    def line_copy(downward, block, j, device):
        cols = pl.ds(j * chunk, chunk)
        return remote(
            onward.at[block, :, cols], from_line.at[downward, block, :, cols],
            line_send.at[block, j], line_recv.at[downward, block, j], device,
        )

    def pick(k):
        block = 0
        for zz in range(lines):
            others = sorted(
                (b for b in range(lines) if b != zz), key=lambda b: (-abs(b - zz), b)
            )
            for kk, b in enumerate(others):
                block = jnp.where((z == zz) & (k == kk), b, block)
        return block

    def cross_copy():
        return remote(x_out, x_in, cross_send, cross_recv, over_x)

    def visit(k, carry):
        block = pick(k)
        downward = jnp.where(block < z, 1, 0)

        @pl.when((k > 0) & ((z == 0) | (z == last)))
        def _():
            for e in range(half):
                distance, part = arrival(PIECES * (lines - 2) + (k - 1) * half + e, last)
                source = jnp.clip(jnp.where(z == 0, distance, last - distance), 0, last)
                tok_copy(source, part, up_send, above).wait_recv()

        activate(block)
        device = at(jnp.clip(jnp.where(downward == 1, z - 1, z + 1), 0, last), y, x, c)
        inner = jnp.where(downward == 1, z < last, z > 0)

        def one(j, carry):
            @pl.when(k == 0)
            def _():
                d_over(j).wait_recv()
                d_plane(j).start()
                d_mate(j, 0).start()
                d_plane(j).wait_recv()
                d_mate(j, 1).start()
                d_mate(j, 0).wait_recv()
                d_mate(j, 1).wait_recv()

            cols = pl.ds(pl.multiple_of(j * chunk, chunk), chunk)
            own = partial(cols)

            @pl.when(inner)
            def _():
                line_copy(downward, block, j, device).wait_recv()

            onward[block, :, cols] = (
                own + from_line[downward, block, :, cols].astype(jnp.float32)
            ).astype(jnp.bfloat16)
            line_copy(downward, block, j, device).start()
            return carry

        lax.fori_loop(0, CHUNKS, one, 0)

        @pl.when(k == 0)
        def _():
            for owner_x in range(TP // CORES):
                pair_copy(owner_x).wait_recv()
            x_out[...] = (keep[1 - x] + mate_in[1 - x].astype(jnp.float32)).astype(jnp.bfloat16)
            cross_copy().start()

        return carry

    lax.fori_loop(0, last, visit, 0)

    activate(z)

    def finish(j, carry):
        cols = pl.ds(pl.multiple_of(j * chunk, chunk), chunk)
        own = partial(cols)

        @pl.when(z > 0)
        def _():
            line_copy(0, z, j, above).wait_recv()

        @pl.when(z < last)
        def _():
            line_copy(1, z, j, above).wait_recv()

        routed_ref[:, cols] = (
            own + from_line[0, z, :, cols].astype(jnp.float32)
            + from_line[1, z, :, cols].astype(jnp.float32)
        ).astype(jnp.bfloat16)
        return carry

    cross_copy().wait_recv()
    attn_ref[...] = (
        keep[x] + mate_in[x].astype(jnp.float32) + x_in[...].astype(jnp.float32)
    ).astype(jnp.bfloat16)
    lax.fori_loop(0, CHUNKS, finish, 0)

    @pl.when(ahead)
    def _():
        halo.wait_send()

    cross_copy().wait_send()
    for owner_x in range(TP // CORES):
        pair_copy(owner_x).wait_send()
    for step in range(1, lines):
        other = lax.rem(z + step, lines)
        share_copy(z, other, at(other, y, x, c)).wait_send()

    def drain_gu(p, carry):
        gu_over(p).wait_send()
        gu_plane(p).wait_send()
        gu_mate(p, 0).wait_send()
        gu_mate(p, 1).wait_send()
        return carry

    lax.fori_loop(0, SLABS, drain_gu, 0)

    def drain_d(p, carry):
        d_over(p).wait_send()
        d_plane(p).wait_send()
        d_mate(p, 0).wait_send()
        d_mate(p, 1).wait_send()
        return carry

    lax.fori_loop(0, CHUNKS, drain_d, 0)

    def drain(line, carry):
        for part in range(PIECES):
            @pl.when((line <= z) & (z < last))
            def _():
                tok_copy(line, part, up_send, above).wait_send()

            @pl.when((line >= z) & (z > 0))
            def _():
                tok_copy(line, part, down_send, below).wait_send()

        @pl.when(line != z)
        def _():
            for j in range(CHUNKS):
                line_copy(0, line, j, above).wait_send()

        return carry

    lax.fori_loop(0, lines, drain, 0)


def fused_layer(normed, shares, gate_weight, up_weight, down_weight, queries, kv_rows, sinks, out_weight):
    lines = lax.axis_size("ep") // ROW
    tok_rows, width = normed.shape
    hidden = gate_weight.shape[1]
    attn_rows, attn_width = queries.shape
    quarter = (attn_rows // TP, out_weight.shape[1])
    block = (tok_rows, width)
    sem = pltpu.SemaphoreType.DMA
    pieces = SLABS + CHUNKS
    bf16, f32 = jnp.bfloat16, jnp.float32
    flops = 12 * lines * tok_rows * width * hidden
    return pl.pallas_call(
        functools.partial(fused_kernel, lines, width),
        out_shape=(jax.ShapeDtypeStruct(block, bf16), jax.ShapeDtypeStruct(quarter, bf16)),
        in_specs=[pl.BlockSpec(memory_space=pl.ANY)] * 9,
        out_specs=(pl.BlockSpec(memory_space=pltpu.VMEM), pl.BlockSpec(memory_space=pltpu.VMEM)),
        scratch_shapes=[
            pltpu.VMEM((lines,) + block, bf16),
            pltpu.VMEM((lines,) + shares.shape, f32),
            pltpu.VMEM((ROW, width, 2 * hidden), bf16),
            pltpu.VMEM((ROW * hidden, width), bf16),
            pltpu.VMEM((ROW, tok_rows, hidden), bf16),
            pltpu.VMEM((lines,) + block, bf16),
            pltpu.VMEM((2, lines) + block, bf16),
            pltpu.VMEM(queries.shape, bf16),
            pltpu.VMEM((attn_rows + WINDOW, kv_rows.shape[1]), bf16),
            pltpu.VMEM(sinks.shape, f32),
            pltpu.VMEM(out_weight.shape, bf16),
            pltpu.VMEM((TP // CORES,) + quarter, f32),
            pltpu.VMEM((TP // CORES,) + quarter, bf16),
            pltpu.VMEM((TP // CORES,) + quarter, bf16),
            pltpu.VMEM(quarter, bf16),
            pltpu.VMEM(quarter, bf16),
            sem((9,)),
            sem((lines,)),
            sem((lines,)),
            sem((2,)),
            sem((lines, PIECES)),
            sem((lines, PIECES)),
            sem((lines, PIECES)),
            sem((pieces,)),
            sem((pieces,)),
            sem((pieces,)),
            sem((pieces,)),
            sem((2, pieces)),
            sem((2, pieces)),
            sem((lines, CHUNKS)),
            sem((2, lines, CHUNKS)),
            sem((TP // CORES,)),
            sem((TP // CORES,)),
            sem,
            sem,
        ],
        compiler_params=pltpu.CompilerParams(
            collective_id=0, has_side_effects=True, vmem_limit_bytes=56 * 1024 * 1024
        ),
        cost_estimate=pl.CostEstimate(
            flops=flops, bytes_accessed=16 * tok_rows * width * lines, transcendentals=0
        ),
    )(normed, shares, gate_weight, up_weight, down_weight, queries, kv_rows, sinks, out_weight)


def fused_path(
    queries, head_keys, head_values, sink_logits, out_weight,
    moe_input, norm_gain, routes, route_weight, gate_weight, up_weight, down_weight,
):
    targets = lax.axis_size("ep")
    values32 = moe_input.astype(jnp.float32)
    scale = lax.rsqrt(jnp.mean(values32 * values32, axis=-1, keepdims=True) + EPSILON)
    normed = (values32 * scale * norm_gain).astype(jnp.bfloat16)
    experts = jnp.arange(targets, dtype=jnp.int32)
    named = routes[:, None, :] == experts[None, :, None]
    shares = jnp.sum(jnp.where(named, route_weight[:, None, :], 0.0), axis=2).T
    kv_rows = jnp.concatenate([head_keys, head_keys, head_values, head_values], axis=1)
    sinks = jnp.broadcast_to(sink_logits[:, None], (sink_logits.shape[0], 128))
    routed, attended = fused_layer(
        normed, shares, gate_weight[0], up_weight[0], down_weight[0], queries, kv_rows, sinks,
        out_weight,
    )
    return (attended, routed)


def fits(queries, head_keys, sink_logits, moe_input, routes):
    targets = lax.axis_size("ep")
    tok_rows = moe_input.shape[0]
    return (
        2 * routes.shape[1] * tok_rows // targets >= tok_rows
        and targets == 4 * ROW
        and lax.axis_size("tp") == TP
        and head_keys.shape[1] == HEAD_DIM
        and sink_logits.shape[0] == 4
        and queries.shape[0] == SLABS * WINDOW
    )


def on_device(
    queries,
    head_keys,
    head_values,
    sink_logits,
    out_weight,
    moe_input,
    norm_gain,
    routes,
    route_weight,
    gate_weight,
    up_weight,
    down_weight,
):
    if fits(queries, head_keys, sink_logits, moe_input, routes):
        return fused_path(
            queries, head_keys, head_values, sink_logits, out_weight, moe_input, norm_gain,
            routes, route_weight, gate_weight, up_weight, down_weight,
        )
    attention_out = attend(queries, head_keys, head_values, sink_logits, out_weight)
    routed_out = experts_part(
        moe_input, norm_gain, routes, route_weight, gate_weight, up_weight, down_weight
    )
    return (attention_out, routed_out)


def solution(mesh):
    placed = (
        P("ep", "tp"),
        P("ep", "tp"),
        P("ep", "tp"),
        P("tp"),
        P("tp", None),
        P(("ep", "tp"), None),
        P(),
        P(("ep", "tp"), None),
        P(("ep", "tp"), None),
        P("ep", None, None),
        P("ep", None, None),
        P("ep", None, None),
    )
    return jax.shard_map(
        on_device,
        mesh=mesh,
        in_specs=placed,
        out_specs=(P(("ep", "tp"), None), P(("ep", "tp"), None)),
        check_vma=False,
    )
```

time: 150 us -> 108 us (0.72)
  the two profiles are of different devices: /device:TPU:0 before, /device:TPU:17 now
where the time goes in v1:
time: 108 us
  Pallas kernels  96 us (89%)
  local copies, waits for them, and re-layouts  6.62 us (6%)
  other arithmetic  4.71 us (4%)
    pallas_call x1, Pallas kernels, fused_layer(): pl.pallas_call(functools.partial(fused_kernel, lines, width), out_shape=(...  96 us
    unnamed x10, local copies, waits for them, and re-layouts  5.31 us

profile of v1, /device:TPU:17, one launch (start us, length us, event | category | flops | bytes accessed | tf_op | source)
XLA Modules:
  0.0 108.0 jit_solution(14934543569142151779)
XLA Ops:
  0.6 0.0 copy-start
  0.6 0.0 copy-start.2
  0.6 1.3 %fusion = f32[128]{0:T(128)S(1)} fusion(bf16[128,2048]{1,0:T(8,128)(2,1)} %param.17), kind=kLoop, calls=%fused_computation.2 | loop fusion | flops 786304 | bytes 524800 | tf_op jit(solution)/shard_map/reduce_sum | solution.py:687
  1.9 1.3 %broadcast_in_dim.16.sinks_hbm = f32[4,128]{1,0:T(4,128)} broadcast(f32[4]{0:T(128)} %param.15), dimensions={0} | broadcast | bytes 2064 | tf_op jit(solution)/shard_map/broadcast_in_dim | solution.py:693
  3.3 1.3 %select_reduce_fusion = f32[128,8]{0,1:T(8,128)} fusion(f32[128,4]{0,1:T(4,128)} %param.20, s32[128,4]{0,1:T(4,128)} %param.19), kind=kLoop, calls=%fused_computation.6 | loop fusion | flops 11264 | bytes 8192 | tf_op jit(solution)/shard_map/reduce_sum | solution.py:691
  4.5 1.1 copy.20
  5.6 1.1 copy.22
  6.7 1.1 %pad_maximum_fusion.kv_hbm = bf16[1024,256]{1,0:T(8,128)(2,1)} fusion(bf16[1024,64]{1,0:T(8,128)(2,1)S(1)} %copy.22, bf16[1024,64]{1,0:T(8,128)(2,1)S(1)} %copy.20), kind=kLoop, calls=%fused_computation.5 | loop fusion | flops 2097152 | bytes 786432 | tf_op jit(solution)/shard_map/concatenate | solution.py:692
  7.9 0.0 copy-done
  7.9 0.0 copy-done.2
  7.9 1.0 fusion.2.rows_hbm
  8.8 96.0 %shard_map.131 = (bf16[128,2048]{1,0:T(8,128)(2,1)}, bf16[256,2048]{1,0:T(8,128)(2,1)}) custom-call(bf16[128,2048]{1,0:T(8,128)(2,1)} %fusion.2.rows_hbm, f32[8,128]{1,0:T(8,128)} %bitcast.4, bf16[2048,512]{1,0:T(8,128)(2,1)} %bitcast.5, bf16[2048,512]{1,0:T(8,128)(2,1)} %bitcast.6, bf16[512,2048]{1,0:T(8,128)(2,1)} %bitcast.7, bf16[1024,256]{1,0:T(8,128)(2,1)} %q_hbm.1, ...), custom_call_target="tpu_custom_call" | custom-call | flops 6442450944 | bytes 16777216 | tf_op jit(solution)/shard_map/pallas_call | solution.py:630
  104.9 0.0 copy-start.1
  104.9 2.4 %copy.26 = bf16[256,2048]{1,0:T(8,128)(2,1)} copy(bf16[256,2048]{1,0:T(8,128)(2,1)} %get-tuple-element.8) | data formatting | bytes 2097152
  107.2 0.0 copy-done.1
  107.2 0.8 copy.27
  (1 shorter events, 0.0 us)
Async XLA Ops:
  0.6 7.2 %copy-start = (bf16[128,2048]{1,0:T(8,128)(2,1)S(1)}, bf16[128,2048]{1,0:T(8,128)(2,1)}, u32[]{:S(2)}) copy-start(bf16[128,2048]{1,0:T(8,128)(2,1)} %param.17) | copy-start | bytes 1572868
  0.6 7.2 %copy-start.2 = (f32[2048]{0:T(1024)S(1)}, f32[2048]{0:T(1024)}, u32[]{:S(2)}) copy-start(f32[2048]{0:T(1024)} %param.18) | copy-start | bytes 24580
  104.9 2.4 %copy-start.1 = (bf16[128,2048]{1,0:T(8,128)(2,1)S(1)}, bf16[128,2048]{1,0:T(8,128)(2,1)}, u32[]{:S(2)}) copy-start(bf16[128,2048]{1,0:T(8,128)(2,1)} %get-tuple-element.9) | copy-start | bytes 1572868

commit v2 on v1

--- a/solution.py
+++ b/solution.py
@@ -136,17 +136,20 @@
 TP = 4
 PIECES = 4
 CHUNKS = 4
-SLABS = 8
-LAG = 2
+SLABS = 16
+LAG = 4
+NORM_ROWS = 16
 
 
 def fused_kernel(
     lines, width,
-    rows_hbm, shares_hbm, gate_hbm, up_hbm, down_hbm, q_hbm, kv_hbm, sinks_hbm, proj_hbm,
+    rows_hbm, gain_hbm, routes_hbm, route_weight_hbm, gate_hbm, up_hbm, down_hbm,
+    q_hbm, keys_hbm, values_hbm, sinks_hbm, proj_hbm,
     routed_ref, attn_ref,
+    raw, gain, routes, route_weight,
     gath, shares, wgu, wd, act, onward, from_line,
     qs, ext, sinks, wo, keep, mate_out, mate_in, x_out, x_in,
-    local_sem, share_send, share_recv, halo_sem,
+    local_sem, gu_sem, share_send, share_recv, halo_sem,
     up_send, down_send, tok_recv,
     y_send, y_recv, x_send, x_recv, m_send, m_recv,
     line_send, line_recv, pair_send, pair_recv, cross_send, cross_recv,
@@ -155,9 +158,12 @@
     z, y, x, c = ep // ROW, ep % ROW, tp // CORES, tp % CORES
     tok_rows, model_width = routed_ref.shape
     hidden = gate_hbm.shape[1]
+    attn_rows = q_hbm.shape[0]
     piece = tok_rows // PIECES
     chunk = model_width // CHUNKS
     last = lines - 1
+    quarter = wgu.shape[1] // TP
+    slab = quarter // SLABS
 
     def at(zz, yy, xx, cc):
         return {"ep": zz * ROW + yy, "tp": xx * CORES + cc}
@@ -172,23 +178,36 @@
     below = at(jnp.maximum(z - 1, 0), y, x, c)
     over_y, over_x, mate = at(z, 1 - y, x, c), at(z, y, 1 - x, c), at(z, y, x, 1 - c)
 
-    own_kv = ext.at[pl.ds(WINDOW, q_hbm.shape[0])]
+    def gu_load(q, half):
+        place = pl.ds(q * quarter, quarter)
+        source = (gate_hbm, up_hbm)[half]
+        return pltpu.make_async_copy(
+            source.at[place], wgu.at[0, place, pl.ds(half * hidden, hidden)], gu_sem.at[half, q]
+        )
+
+    own = pl.ds(WINDOW, attn_rows)
     loads = [
         pltpu.make_async_copy(source, target, local_sem.at[i])
         for i, (source, target) in enumerate([
-            (kv_hbm, own_kv),
-            (rows_hbm, gath.at[z]),
-            (shares_hbm, shares.at[z]),
-            (gate_hbm, wgu.at[0, :, pl.ds(0, hidden)]),
-            (up_hbm, wgu.at[0, :, pl.ds(hidden, hidden)]),
+            (keys_hbm, ext.at[pl.ds(0, HEAD_DIM), own]),
+            (values_hbm, ext.at[pl.ds(HEAD_DIM, HEAD_DIM), own]),
+            (rows_hbm, raw),
+            (gain_hbm, gain),
+            (routes_hbm, routes),
+            (route_weight_hbm, route_weight),
             (down_hbm, wd.at[pl.ds(0, hidden)]),
             (q_hbm, qs),
             (sinks_hbm, sinks),
             (proj_hbm, wo),
         ])
     ]
+    gu_load(tp, 0).start()
+    gu_load(tp, 1).start()
     for load in loads:
         load.start()
+    for step in range(1, TP):
+        gu_load(lax.rem(tp + step, TP), 0).start()
+        gu_load(lax.rem(tp + step, TP), 1).start()
 
     ahead = ep + 1 < lines * ROW
     behind = ep > 0
@@ -212,7 +231,7 @@
     pl.semaphore_wait(barrier, last + 3 + jnp.where(skew, 1, 0))
 
     halo = remote(
-        ext.at[pl.ds(q_hbm.shape[0], WINDOW)], ext.at[pl.ds(0, WINDOW)], halo_sem.at[0],
+        ext.at[:, pl.ds(attn_rows, WINDOW)], ext.at[:, pl.ds(0, WINDOW)], halo_sem.at[0],
         halo_sem.at[1], {"ep": jnp.minimum(ep + 1, lines * ROW - 1), "tp": tp},
     )
 
@@ -224,9 +243,6 @@
     def tok_copy(block, part, sems, device):
         view = gath.at[block, pl.ds(part * piece, piece)]
         return remote(view, view, sems.at[block, part], tok_recv.at[block, part], device)
-
-    quarter = wgu.shape[1] // TP
-    slab = quarter // SLABS
 
     def gu_view(expert, q, p):
         return wgu.at[expert, pl.ds(q * quarter + p * slab, slab)]
@@ -260,16 +276,38 @@
     d_over, d_plane, d_mate = weight_copies(d_view, SLABS)
 
     loads[0].wait()
+    loads[1].wait()
 
     @pl.when(ahead)
     def _():
         halo.start()
 
-    loads[1].wait()
-    loads[2].wait()
-    for step in range(1, lines):
-        other = lax.rem(z + step, lines)
-        share_copy(z, other, at(other, y, x, c)).start()
+    gu_load(tp, 0).wait()
+    gu_load(tp, 1).wait()
+
+    def launch_gu(p, carry):
+        gu_over(p).start()
+        return carry
+
+    lax.fori_loop(0, SLABS, launch_gu, 0)
+    for load in loads[2:6]:
+        load.wait()
+
+    def normalize(i, carry):
+        place = pl.ds(i * NORM_ROWS, NORM_ROWS)
+        values32 = raw[place].astype(jnp.float32)
+        mean = jnp.sum(values32 * values32, axis=-1, keepdims=True) * (1.0 / model_width)
+        scale = lax.rsqrt(mean + EPSILON)
+        gath[z, place] = (values32 * scale * gain[...]).astype(jnp.bfloat16)
+        return carry
+
+    lax.fori_loop(0, tok_rows // NORM_ROWS, normalize, 0)
+    expert = lax.broadcasted_iota(jnp.int32, shares.shape[1:], 0)
+    share = jnp.zeros(shares.shape[1:], jnp.float32)
+    for choice in range(routes.shape[0]):
+        named = routes[choice : choice + 1, :] == expert
+        share = share + jnp.where(named, route_weight[choice : choice + 1, :], 0.0)
+    shares[z] = share
 
     def own_tokens(first, count, upward):
         for part in range(first, first + count):
@@ -296,41 +334,18 @@
     def _():
         own_tokens(half, half, False)
 
-    loads[3].wait()
-    loads[4].wait()
-
-    def launch_gu(p, carry):
-        gu_over(p).start()
-        return carry
-
-    lax.fori_loop(0, SLABS, launch_gu, 0)
-    loads[5].wait()
+    for step in range(1, lines):
+        other = lax.rem(z + step, lines)
+        share_copy(z, other, at(other, y, x, c)).start()
+    loads[6].wait()
 
     def launch_d(p, carry):
         d_over(p).start()
         return carry
 
     lax.fori_loop(0, CHUNKS, launch_d, 0)
-
-    @pl.when(z == 0)
-    def _():
-        from_line[0] = jnp.zeros_like(from_line[0])
-
-    @pl.when(z == last)
-    def _():
-        from_line[1] = jnp.zeros_like(from_line[1])
-
-    loads[6].wait()
-    loads[7].wait()
-    loads[8].wait()
-
-    @pl.when(behind)
-    def _():
-        halo.wait_recv()
-
-    @pl.when(ep == 0)
-    def _():
-        ext[pl.ds(0, WINDOW)] = jnp.zeros((WINDOW, ext.shape[1]), ext.dtype)
+    for load in loads[7:]:
+        load.wait()
 
     def arrival(i, reach):
         s = i // half
@@ -364,7 +379,6 @@
     band = 2 * WINDOW
     quarter_rows = attn_ref.shape[0]
     blocks_each = quarter_rows // WINDOW
-    kv_width = ext.shape[1] // 2
 
     def pair_copy(owner_x):
         return remote(
@@ -374,17 +388,15 @@
 
     def attend_block(n):
         q_rows = qs[pl.ds(n * WINDOW, WINDOW)] * jnp.bfloat16(HEAD_DIM ** (-0.5))
-        held = ext[pl.ds(n * WINDOW, band)]
-        keys = jnp.concatenate([held[:, :kv_width]] * 2, axis=1)
-        values = jnp.concatenate([held[:, kv_width:]] * 2, axis=1)
+        held = ext[:, pl.ds(pl.multiple_of(n * WINDOW, WINDOW), band)]
+        keys = jnp.concatenate([held[:HEAD_DIM]] * per_group, axis=0)
+        values = held[HEAD_DIM:]
         q_head = lax.broadcasted_iota(jnp.int32, q_rows.shape, 1) // HEAD_DIM
         stacked = jnp.concatenate(
             [jnp.where(q_head == h, q_rows, jnp.zeros_like(q_rows)) for h in range(per_group)],
             axis=0,
         )
-        scores = lax.dot_general(
-            stacked, keys, (((1,), (1,)), ((), ())), preferred_element_type=jnp.float32
-        )
+        scores = jnp.dot(stacked, keys, preferred_element_type=jnp.float32)
         begins = lax.rem(ep * (qs.shape[0] // WINDOW) + n, lines * ROW * (qs.shape[0] // WINDOW) // SEQS) == 0
         row = lax.broadcasted_iota(jnp.int32, (WINDOW, band), 0)
         col = lax.broadcasted_iota(jnp.int32, (WINDOW, band), 1)
@@ -392,18 +404,22 @@
         weights = []
         for h in range(per_group):
             score = jnp.where(valid, scores[h * WINDOW : (h + 1) * WINDOW], NEGATIVE)
-            sink = sinks[h : h + 1, 0:1]
+            sink = sinks[h]
             top = jnp.maximum(jnp.max(score, axis=1, keepdims=True), sink)
             powers = jnp.exp(score - top)
             total = jnp.sum(powers, axis=1, keepdims=True) + jnp.exp(sink - top)
             weights.append((powers * (1.0 / total)).astype(jnp.bfloat16))
-        v_head = lax.broadcasted_iota(jnp.int32, values.shape, 1) // HEAD_DIM
+        blank = jnp.zeros_like(values)
         spread = jnp.concatenate(
-            [jnp.where(v_head == h, values, jnp.zeros_like(values)) for h in range(per_group)],
+            [
+                jnp.concatenate([values if g == h else blank for g in range(per_group)], axis=1)
+                for h in range(per_group)
+            ],
             axis=0,
         )
-        heads = jnp.dot(
-            jnp.concatenate(weights, axis=1), spread, preferred_element_type=jnp.float32
+        heads = lax.dot_general(
+            jnp.concatenate(weights, axis=1), spread, (((1,), (1,)), ((), ())),
+            preferred_element_type=jnp.float32,
         ).astype(jnp.bfloat16)
         owner = n // blocks_each
         owner_x, owner_c = owner // CORES, owner % CORES
@@ -418,41 +434,75 @@
         def _():
             mate_out[owner_x, place] = share.astype(jnp.bfloat16)
 
+    each = SLABS * WINDOW // attn_rows
+
     def slot(i, carry):
         gu_over(i).wait_recv()
         gu_plane(i).start()
         gu_mate(i, 0).start()
-        pump_tokens(i)
 
         @pl.when(i >= LAG)
         def _():
             gu_plane(i - LAG).wait_recv()
             gu_mate(i - LAG, 1).start()
 
-        attend_block(i)
+        @pl.when(i % each == 0)
+        def _():
+            n = lax.rem(i // each + 1, attn_rows // WINDOW)
+
+            @pl.when((n == 0) & behind)
+            def _():
+                halo.wait_recv()
+
+            @pl.when((n == 0) & (ep == 0))
+            def _():
+                ext[:, pl.ds(0, WINDOW)] = jnp.zeros((ext.shape[0], WINDOW), ext.dtype)
+
+            attend_block(n)
+
+        @pl.when(i % each == each - 1)
+        def _():
+            pump_tokens(i // each)
+
+        @pl.when((i % each == each - 1) & (i // each < lines))
+        def _():
+            block = jnp.minimum(i // each, last)
+
+            @pl.when(z == 0)
+            def _():
+                from_line[0, block] = jnp.zeros(from_line.shape[2:], from_line.dtype)
+
+            @pl.when(z == last)
+            def _():
+                from_line[1, block] = jnp.zeros(from_line.shape[2:], from_line.dtype)
+
         return carry
 
     lax.fori_loop(0, SLABS, slot, 0)
     for owner_x in range(TP // CORES):
         pair_copy(owner_x).start()
+
+    def pass_down(j):
+        d_over(j).wait_recv()
+        d_plane(j).start()
+        d_mate(j, 0).start()
+
     for p in range(SLABS - LAG, SLABS):
+        if p == SLABS - LAG // 2:
+            pass_down(0)
         gu_plane(p).wait_recv()
         gu_mate(p, 1).start()
     for step in range(1, lines):
         source = lax.rem(z + step, lines)
         share_copy(source, source, at(source, y, x, c)).wait_recv()
-
-    def gather_gu(p, carry):
-        gu_mate(p, 0).wait_recv()
-        gu_mate(p, 1).wait_recv()
-        return carry
-
-    lax.fori_loop(0, SLABS, gather_gu, 0)
+    for step in range(1, TP):
+        gu_load(lax.rem(tp + step, TP), 0).wait()
+        gu_load(lax.rem(tp + step, TP), 1).wait()
 
     square = (tok_rows, tok_rows)
     eye = lax.broadcasted_iota(jnp.int32, square, 0) == lax.broadcasted_iota(jnp.int32, square, 1)
 
-    def activate(block):
+    def activate(block, first, end):
         def one(expert, carry):
             pre = jnp.dot(gath[block], wgu[expert], preferred_element_type=jnp.float32)
             unit = clamped_unit(pre[:, :hidden], pre[:, hidden:])
@@ -463,7 +513,7 @@
             act[expert] = (unit * column).astype(jnp.bfloat16)
             return carry
 
-        lax.fori_loop(0, ROW, one, 0)
+        lax.fori_loop(first, end, one, 0)
 
     def partial(cols):
         both = jnp.concatenate([act[0], act[1]], axis=1)
@@ -480,7 +530,8 @@
         block = 0
         for zz in range(lines):
             others = sorted(
-                (b for b in range(lines) if b != zz), key=lambda b: (-abs(b - zz), b)
+                (b for b in range(lines) if b != zz),
+                key=lambda b: (-abs(b - zz), min(b, last - b)),
             )
             for kk, b in enumerate(others):
                 block = jnp.where((z == zz) & (k == kk), b, block)
@@ -500,16 +551,17 @@
                 source = jnp.clip(jnp.where(z == 0, distance, last - distance), 0, last)
                 tok_copy(source, part, up_send, above).wait_recv()
 
-        activate(block)
+        activate(block, jnp.where(k == 0, 1, 0), ROW)
         device = at(jnp.clip(jnp.where(downward == 1, z - 1, z + 1), 0, last), y, x, c)
         inner = jnp.where(downward == 1, z < last, z > 0)
 
         def one(j, carry):
             @pl.when(k == 0)
             def _():
-                d_over(j).wait_recv()
-                d_plane(j).start()
-                d_mate(j, 0).start()
+                @pl.when(j + 2 < CHUNKS)
+                def _():
+                    pass_down(jnp.minimum(j + 2, CHUNKS - 1))
+
                 d_plane(j).wait_recv()
                 d_mate(j, 1).start()
                 d_mate(j, 0).wait_recv()
@@ -526,22 +578,32 @@
                 own + from_line[downward, block, :, cols].astype(jnp.float32)
             ).astype(jnp.bfloat16)
             line_copy(downward, block, j, device).start()
+
+            @pl.when((k == 0) & (j == CHUNKS - 3))
+            def _():
+                for owner_x in range(TP // CORES):
+                    pair_copy(owner_x).wait_recv()
+                x_out[...] = (
+                    keep[1 - x] + mate_in[1 - x].astype(jnp.float32)
+                ).astype(jnp.bfloat16)
+                cross_copy().start()
+
             return carry
 
         lax.fori_loop(0, CHUNKS, one, 0)
-
-        @pl.when(k == 0)
-        def _():
-            for owner_x in range(TP // CORES):
-                pair_copy(owner_x).wait_recv()
-            x_out[...] = (keep[1 - x] + mate_in[1 - x].astype(jnp.float32)).astype(jnp.bfloat16)
-            cross_copy().start()
-
-        return carry
-
+        return carry
+
+    pass_down(1)
+    activate(pick(0), 0, 1)
+
+    def gather_gu(p, carry):
+        gu_mate(p, 0).wait_recv()
+        gu_mate(p, 1).wait_recv()
+        return carry
+
+    lax.fori_loop(0, SLABS, gather_gu, 0)
     lax.fori_loop(0, last, visit, 0)
-
-    activate(z)
+    activate(z, 0, ROW)
 
     def finish(j, carry):
         cols = pl.ds(pl.multiple_of(j * chunk, chunk), chunk)
@@ -616,11 +678,13 @@
     lax.fori_loop(0, lines, drain, 0)
 
 
-def fused_layer(normed, shares, gate_weight, up_weight, down_weight, queries, kv_rows, sinks, out_weight):
-    lines = lax.axis_size("ep") // ROW
-    tok_rows, width = normed.shape
+def fused_layer(*operands):
+    moe_input, _, routes, _, gate_weight, _, _, queries, keys, _, sinks, out_weight = operands
+    targets = lax.axis_size("ep")
+    lines = targets // ROW
+    tok_rows, width = moe_input.shape
     hidden = gate_weight.shape[1]
-    attn_rows, attn_width = queries.shape
+    attn_rows = queries.shape[0]
     quarter = (attn_rows // TP, out_weight.shape[1])
     block = (tok_rows, width)
     sem = pltpu.SemaphoreType.DMA
@@ -629,27 +693,32 @@
     flops = 12 * lines * tok_rows * width * hidden
     return pl.pallas_call(
         functools.partial(fused_kernel, lines, width),
-        out_shape=(jax.ShapeDtypeStruct(block, bf16), jax.ShapeDtypeStruct(quarter, bf16)),
-        in_specs=[pl.BlockSpec(memory_space=pl.ANY)] * 9,
+        out_shape=(pltpu.VMEM(block, bf16), pltpu.VMEM(quarter, bf16)),
+        in_specs=[pl.BlockSpec(memory_space=pl.ANY)] * len(operands),
         out_specs=(pl.BlockSpec(memory_space=pltpu.VMEM), pl.BlockSpec(memory_space=pltpu.VMEM)),
         scratch_shapes=[
+            pltpu.VMEM(block, bf16),
+            pltpu.VMEM((1, width), f32),
+            pltpu.VMEM(routes.shape, jnp.int32),
+            pltpu.VMEM(routes.shape, f32),
             pltpu.VMEM((lines,) + block, bf16),
-            pltpu.VMEM((lines,) + shares.shape, f32),
+            pltpu.VMEM((lines, targets, tok_rows), f32),
             pltpu.VMEM((ROW, width, 2 * hidden), bf16),
             pltpu.VMEM((ROW * hidden, width), bf16),
             pltpu.VMEM((ROW, tok_rows, hidden), bf16),
             pltpu.VMEM((lines,) + block, bf16),
             pltpu.VMEM((2, lines) + block, bf16),
             pltpu.VMEM(queries.shape, bf16),
-            pltpu.VMEM((attn_rows + WINDOW, kv_rows.shape[1]), bf16),
-            pltpu.VMEM(sinks.shape, f32),
+            pltpu.VMEM((2 * HEAD_DIM, WINDOW + attn_rows), bf16),
+            pltpu.SMEM(sinks.shape, f32),
             pltpu.VMEM(out_weight.shape, bf16),
             pltpu.VMEM((TP // CORES,) + quarter, f32),
             pltpu.VMEM((TP // CORES,) + quarter, bf16),
             pltpu.VMEM((TP // CORES,) + quarter, bf16),
             pltpu.VMEM(quarter, bf16),
             pltpu.VMEM(quarter, bf16),
-            sem((9,)),
+            sem((10,)),
+            sem((2, TP)),
             sem((lines,)),
             sem((lines,)),
             sem((2,)),
@@ -675,25 +744,17 @@
         cost_estimate=pl.CostEstimate(
             flops=flops, bytes_accessed=16 * tok_rows * width * lines, transcendentals=0
         ),
-    )(normed, shares, gate_weight, up_weight, down_weight, queries, kv_rows, sinks, out_weight)
+    )(*operands)
 
 
 def fused_path(
     queries, head_keys, head_values, sink_logits, out_weight,
     moe_input, norm_gain, routes, route_weight, gate_weight, up_weight, down_weight,
 ):
-    targets = lax.axis_size("ep")
-    values32 = moe_input.astype(jnp.float32)
-    scale = lax.rsqrt(jnp.mean(values32 * values32, axis=-1, keepdims=True) + EPSILON)
-    normed = (values32 * scale * norm_gain).astype(jnp.bfloat16)
-    experts = jnp.arange(targets, dtype=jnp.int32)
-    named = routes[:, None, :] == experts[None, :, None]
-    shares = jnp.sum(jnp.where(named, route_weight[:, None, :], 0.0), axis=2).T
-    kv_rows = jnp.concatenate([head_keys, head_keys, head_values, head_values], axis=1)
-    sinks = jnp.broadcast_to(sink_logits[:, None], (sink_logits.shape[0], 128))
     routed, attended = fused_layer(
-        normed, shares, gate_weight[0], up_weight[0], down_weight[0], queries, kv_rows, sinks,
-        out_weight,
+        moe_input, norm_gain.reshape(1, -1), routes.T, route_weight.T,
+        gate_weight[0], up_weight[0], down_weight[0],
+        queries, head_keys.T, head_values.T, sink_logits, out_weight,
     )
     return (attended, routed)
 
@@ -707,7 +768,8 @@
         and lax.axis_size("tp") == TP
         and head_keys.shape[1] == HEAD_DIM
         and sink_logits.shape[0] == 4
-        and queries.shape[0] == SLABS * WINDOW
+        and (SLABS * WINDOW) % queries.shape[0] == 0
+        and queries.shape[0] >= 4 * ROW * WINDOW
     )
 
 

time: 108 us -> 80 us (0.74)
  Pallas kernels: 96 us -> 76.6 us
  local copies, waits for them, and re-layouts: 6.62 us -> 1.77 us
  other arithmetic: 4.71 us -> 0 us
    pallas_call x1, Pallas kernels: 96 us -> 76.6 us  [fused_layer(): pl.pallas_call(functools.partial(fused_kernel, lines, width), out_shape=(...]
    unnamed x10 -> x2, local copies, waits for them, and re-layouts: 5.31 us -> 1.77 us
    reduce_sum x2 -> x0, other arithmetic: 2.58 us -> none  [the longest x1 1.3 us: fused_path(): shares = jnp.sum(jnp.where(named, route_weight[:, None, :], 0.0), axis=2).T]
    broadcast_in_dim x1 -> x0, local copies, waits for them, and re-layouts: 1.31 us -> none  [fused_path(): sinks = jnp.broadcast_to(sink_logits[:, None], (sink_logits.shape[0], 128))]
    concatenate x1 -> x0, other arithmetic: 1.14 us -> none  [fused_path(): jnp.concatenate([head_keys, head_keys, head_values, head_values], axis=1)]
where the time goes in v2:
time: 80 us; the launch traced here: 79 us
  Pallas kernels  76.6 us (96%)
  local copies, waits for them, and re-layouts  1.77 us (2%)
    pallas_call x1, Pallas kernels, fused_layer(): pl.pallas_call(functools.partial(fused_kernel, lines, width), out_shape=(...  76.6 us
    unnamed x2, local copies, waits for them, and re-layouts  1.77 us

profile of v2, /device:TPU:17, one launch (start us, length us, event | category | flops | bytes accessed | tf_op | source)
XLA Modules:
  0.0 79.0 jit_solution(171748520642518071)
XLA Ops:
  0.6 76.6 %shard_map.131 = (bf16[128,2048]{1,0:T(8,128)(2,1)S(1)}, bf16[256,2048]{1,0:T(8,128)(2,1)S(1)}) custom-call(bf16[128,2048]{1,0:T(8,128)(2,1)} %rows_hbm.1, f32[1,2048]{1,0:T(1,128)} %bitcast.13, s32[4,128]{1,0:T(4,128)} %bitcast.14, f32[4,128]{1,0:T(4,128)} %bitcast.15, bf16[2048,512]{1,0:T(8,128)(2,1)} %bitcast.8, bf16[2048,512]{1,0:T(8,128)(2,1)} %bitcast.9, ...), custom_call_target="tpu_custom_call" | custom-call | flops 6442450944 | bytes 16777216 | tf_op jit(solution)/shard_map/pallas_call | solution.py:694
  77.2 1.0 %copy.16 = bf16[256,2048]{1,0:T(8,128)(2,1)} copy(bf16[256,2048]{1,0:T(8,128)(2,1)S(1)} %get-tuple-element.6) | data formatting | bytes 2097152
  78.2 0.8 %copy.17 = bf16[128,2048]{1,0:T(8,128)(2,1)} copy(bf16[128,2048]{1,0:T(8,128)(2,1)S(1)} %get-tuple-element.7) | data formatting | bytes 1048576

commit v3 on v2

--- a/solution.py
+++ b/solution.py
@@ -135,9 +135,10 @@
 CORES = 2
 TP = 4
 PIECES = 4
-CHUNKS = 4
+CHUNKS = 8
 SLABS = 16
 LAG = 4
+AHEAD = 3
 NORM_ROWS = 16
 
 
@@ -149,10 +150,10 @@
     raw, gain, routes, route_weight,
     gath, shares, wgu, wd, act, onward, from_line,
     qs, ext, sinks, wo, keep, mate_out, mate_in, x_out, x_in,
-    local_sem, gu_sem, share_send, share_recv, halo_sem,
+    local_sem, gu_sem, share_sem, halo_sem,
     up_send, down_send, tok_recv,
-    y_send, y_recv, x_send, x_recv, m_send, m_recv,
-    line_send, line_recv, pair_send, pair_recv, cross_send, cross_recv,
+    y_send, y_recv, x_send, x_recv, m_send, gm_recv, m_recv,
+    line_send, line_recv, pair_sem, cross_send, cross_recv,
 ):
     ep, tp = lax.axis_index("ep"), lax.axis_index("tp")
     z, y, x, c = ep // ROW, ep % ROW, tp // CORES, tp % CORES
@@ -182,12 +183,16 @@
         place = pl.ds(q * quarter, quarter)
         source = (gate_hbm, up_hbm)[half]
         return pltpu.make_async_copy(
-            source.at[place], wgu.at[0, place, pl.ds(half * hidden, hidden)], gu_sem.at[half, q]
+            source.at[place], wgu.at[0, place, pl.ds(half * hidden, hidden)],
+            gu_sem.at[jnp.where(q == tp, 0, 1)],
         )
+
+    def loaded(target, semaphore):
+        pltpu.make_async_copy(target, target, semaphore).wait()
 
     own = pl.ds(WINDOW, attn_rows)
     loads = [
-        pltpu.make_async_copy(source, target, local_sem.at[i])
+        pltpu.make_async_copy(source, target, local_sem.at[max(i - 1, 0)])
         for i, (source, target) in enumerate([
             (keys_hbm, ext.at[pl.ds(0, HEAD_DIM), own]),
             (values_hbm, ext.at[pl.ds(HEAD_DIM, HEAD_DIM), own]),
@@ -235,14 +240,20 @@
         halo_sem.at[1], {"ep": jnp.minimum(ep + 1, lines * ROW - 1), "tp": tp},
     )
 
-    def share_copy(slot, recv_slot, device):
+    def share_copy(slot, device):
         return remote(
-            shares.at[slot], shares.at[slot], share_send.at[recv_slot], share_recv.at[slot], device
+            shares.at[slot], shares.at[slot], share_sem.at[0], share_sem.at[1], device
         )
+
+    def all_of(view, send, recv):
+        return remote(view, view, send, recv, mate)
+
+    def shares_done():
+        return all_of(shares.at[pl.ds(0, last)], share_sem.at[0], share_sem.at[1])
 
     def tok_copy(block, part, sems, device):
         view = gath.at[block, pl.ds(part * piece, piece)]
-        return remote(view, view, sems.at[block, part], tok_recv.at[block, part], device)
+        return remote(view, view, sems.at[block], tok_recv.at[block, part], device)
 
     def gu_view(expert, q, p):
         return wgu.at[expert, pl.ds(q * quarter + p * slab, slab)]
@@ -252,38 +263,39 @@
             pl.ds(expert * hidden + q * (hidden // TP), hidden // TP), pl.ds(p * chunk, chunk)
         ]
 
-    def weight_copies(view, base):
+    def weight_copies(view, kind, base, mate_recv):
         def over_link(p):
             return remote(
-                view(0, tp, p), view(1, tp, p), y_send.at[base + p], y_recv.at[base + p], over_y
+                view(0, tp, p), view(1, tp, p), y_send.at[kind], y_recv.at[base + p], over_y
             )
 
         def to_plane(p):
             return remote(
-                view(1, tp, p), view(1, tp, p), x_send.at[base + p], x_recv.at[base + p], over_x
+                view(1, tp, p), view(1, tp, p), x_send.at[kind], x_recv.at[base + p], over_x
             )
 
         def to_mate(p, second):
-            q = jnp.where(second == 1, (1 - x) * CORES + c, tp) if second else tp
+            q = (1 - x) * CORES + c if second else tp
             return remote(
-                view(1, q, p), view(1, q, p), m_send.at[second, base + p],
-                m_recv.at[second, base + p], mate,
+                view(1, q, p), view(1, q, p), m_send.at[kind, second], mate_recv(second, p), mate
             )
 
         return over_link, to_plane, to_mate
 
-    gu_over, gu_plane, gu_mate = weight_copies(gu_view, 0)
-    d_over, d_plane, d_mate = weight_copies(d_view, SLABS)
-
-    loads[0].wait()
-    loads[1].wait()
+    gu_over, gu_plane, gu_mate = weight_copies(gu_view, 0, 0, lambda second, p: gm_recv.at[second])
+    d_over, d_plane, d_mate = weight_copies(
+        d_view, 1, SLABS, lambda second, p: m_recv.at[second, p]
+    )
+    gu_whole = wgu.at[1, pl.ds(0, quarter)]
+    d_whole = wd.at[pl.ds(0, hidden // TP)]
+
+    loaded(ext.at[:, own], local_sem.at[0])
 
     @pl.when(ahead)
     def _():
         halo.start()
 
-    gu_load(tp, 0).wait()
-    gu_load(tp, 1).wait()
+    loaded(wgu.at[0, pl.ds(0, quarter)], gu_sem.at[0])
 
     def launch_gu(p, carry):
         gu_over(p).start()
@@ -336,7 +348,7 @@
 
     for step in range(1, lines):
         other = lax.rem(z + step, lines)
-        share_copy(z, other, at(other, y, x, c)).start()
+        share_copy(z, at(other, y, x, c)).start()
     loads[6].wait()
 
     def launch_d(p, carry):
@@ -382,8 +394,7 @@
 
     def pair_copy(owner_x):
         return remote(
-            mate_out.at[owner_x], mate_in.at[owner_x], pair_send.at[owner_x],
-            pair_recv.at[owner_x], mate,
+            mate_out.at[owner_x], mate_in.at[owner_x], pair_sem.at[0], pair_sem.at[1], mate
         )
 
     def attend_block(n):
@@ -487,17 +498,13 @@
         d_plane(j).start()
         d_mate(j, 0).start()
 
-    for p in range(SLABS - LAG, SLABS):
-        if p == SLABS - LAG // 2:
-            pass_down(0)
+    def late(p, carry):
         gu_plane(p).wait_recv()
         gu_mate(p, 1).start()
-    for step in range(1, lines):
-        source = lax.rem(z + step, lines)
-        share_copy(source, source, at(source, y, x, c)).wait_recv()
-    for step in range(1, TP):
-        gu_load(lax.rem(tp + step, TP), 0).wait()
-        gu_load(lax.rem(tp + step, TP), 1).wait()
+        return carry
+
+    shares_done().wait_recv()
+    loaded(wgu.at[0, pl.ds(quarter, (TP - 1) * quarter)], gu_sem.at[1])
 
     square = (tok_rows, tok_rows)
     eye = lax.broadcasted_iota(jnp.int32, square, 0) == lax.broadcasted_iota(jnp.int32, square, 1)
@@ -519,11 +526,12 @@
         both = jnp.concatenate([act[0], act[1]], axis=1)
         return jnp.dot(both, wd[:, cols], preferred_element_type=jnp.float32)
 
-    def line_copy(downward, block, j, device):
+    def line_copy(downward, block, j, device, holder):
         cols = pl.ds(j * chunk, chunk)
+        row = jnp.where(downward == 1, lines - holder + block, block - holder)
         return remote(
             onward.at[block, :, cols], from_line.at[downward, block, :, cols],
-            line_send.at[block, j], line_recv.at[downward, block, j], device,
+            line_send.at[block], line_recv.at[row, j], device,
         )
 
     def pick(k):
@@ -540,30 +548,32 @@
     def cross_copy():
         return remote(x_out, x_in, cross_send, cross_recv, over_x)
 
+    edge = (z == 0) | (z == last)
+
+    def send_cross():
+        all_of(mate_in, pair_sem.at[0], pair_sem.at[1]).wait_recv()
+        x_out[...] = (keep[1 - x] + mate_in[1 - x].astype(jnp.float32)).astype(jnp.bfloat16)
+        cross_copy().start()
+
     def visit(k, carry):
         block = pick(k)
         downward = jnp.where(block < z, 1, 0)
 
-        @pl.when((k > 0) & ((z == 0) | (z == last)))
+        @pl.when((k > 0) & edge)
         def _():
             for e in range(half):
                 distance, part = arrival(PIECES * (lines - 2) + (k - 1) * half + e, last)
                 source = jnp.clip(jnp.where(z == 0, distance, last - distance), 0, last)
                 tok_copy(source, part, up_send, above).wait_recv()
 
-        activate(block, jnp.where(k == 0, 1, 0), ROW)
-        device = at(jnp.clip(jnp.where(downward == 1, z - 1, z + 1), 0, last), y, x, c)
+        activate(block, jnp.where(k == 0, ROW, 0), ROW)
+        onto = jnp.clip(jnp.where(downward == 1, z - 1, z + 1), 0, last)
+        device = at(onto, y, x, c)
         inner = jnp.where(downward == 1, z < last, z > 0)
 
         def one(j, carry):
             @pl.when(k == 0)
             def _():
-                @pl.when(j + 2 < CHUNKS)
-                def _():
-                    pass_down(jnp.minimum(j + 2, CHUNKS - 1))
-
-                d_plane(j).wait_recv()
-                d_mate(j, 1).start()
                 d_mate(j, 0).wait_recv()
                 d_mate(j, 1).wait_recv()
 
@@ -572,36 +582,51 @@
 
             @pl.when(inner)
             def _():
-                line_copy(downward, block, j, device).wait_recv()
+                line_copy(downward, block, j, device, z).wait_recv()
 
             onward[block, :, cols] = (
                 own + from_line[downward, block, :, cols].astype(jnp.float32)
             ).astype(jnp.bfloat16)
-            line_copy(downward, block, j, device).start()
-
-            @pl.when((k == 0) & (j == CHUNKS - 3))
-            def _():
-                for owner_x in range(TP // CORES):
-                    pair_copy(owner_x).wait_recv()
-                x_out[...] = (
-                    keep[1 - x] + mate_in[1 - x].astype(jnp.float32)
-                ).astype(jnp.bfloat16)
-                cross_copy().start()
+            line_copy(downward, block, j, device, onto).start()
+
+            @pl.when((k == 0) & edge & (j + AHEAD < CHUNKS))
+            def _():
+                pass_down(jnp.minimum(j + AHEAD, CHUNKS - 1))
+
+            @pl.when((k == 0) & (j + 1 < CHUNKS))
+            def _():
+                take_plane(jnp.minimum(j + 1, CHUNKS - 1))
+
+            @pl.when((k == 0) & (j == CHUNKS - AHEAD - 1) & edge)
+            def _():
+                send_cross()
 
             return carry
 
         lax.fori_loop(0, CHUNKS, one, 0)
         return carry
 
-    pass_down(1)
+    def take_plane(j):
+        d_plane(j).wait_recv()
+        d_mate(j, 1).start()
+
     activate(pick(0), 0, 1)
-
-    def gather_gu(p, carry):
-        gu_mate(p, 0).wait_recv()
-        gu_mate(p, 1).wait_recv()
-        return carry
-
-    lax.fori_loop(0, SLABS, gather_gu, 0)
+    pass_down(0)
+    lax.fori_loop(SLABS - LAG, SLABS, late, 0)
+    for p in range(1, AHEAD - 1):
+        pass_down(p)
+    for second in range(2):
+        all_of(gu_whole, gm_recv.at[second], gm_recv.at[second]).wait_recv()
+    activate(pick(0), 1, ROW)
+    take_plane(0)
+    pass_down(AHEAD - 1)
+
+    @pl.when(jnp.logical_not(edge))
+    def _():
+        for p in range(AHEAD, CHUNKS):
+            pass_down(p)
+        send_cross()
+
     lax.fori_loop(0, last, visit, 0)
     activate(z, 0, ROW)
 
@@ -611,11 +636,11 @@
 
         @pl.when(z > 0)
         def _():
-            line_copy(0, z, j, above).wait_recv()
+            line_copy(0, z, j, above, z).wait_recv()
 
         @pl.when(z < last)
         def _():
-            line_copy(1, z, j, above).wait_recv()
+            line_copy(1, z, j, above, z).wait_recv()
 
         routed_ref[:, cols] = (
             own + from_line[0, z, :, cols].astype(jnp.float32)
@@ -623,55 +648,37 @@
         ).astype(jnp.bfloat16)
         return carry
 
+    keep[x] = keep[x] + mate_in[x].astype(jnp.float32)
+    lax.fori_loop(0, CHUNKS, finish, 0)
     cross_copy().wait_recv()
-    attn_ref[...] = (
-        keep[x] + mate_in[x].astype(jnp.float32) + x_in[...].astype(jnp.float32)
-    ).astype(jnp.bfloat16)
-    lax.fori_loop(0, CHUNKS, finish, 0)
+    attn_ref[...] = (keep[x] + x_in[...].astype(jnp.float32)).astype(jnp.bfloat16)
 
     @pl.when(ahead)
     def _():
         halo.wait_send()
 
     cross_copy().wait_send()
-    for owner_x in range(TP // CORES):
-        pair_copy(owner_x).wait_send()
-    for step in range(1, lines):
-        other = lax.rem(z + step, lines)
-        share_copy(z, other, at(other, y, x, c)).wait_send()
-
-    def drain_gu(p, carry):
-        gu_over(p).wait_send()
-        gu_plane(p).wait_send()
-        gu_mate(p, 0).wait_send()
-        gu_mate(p, 1).wait_send()
-        return carry
-
-    lax.fori_loop(0, SLABS, drain_gu, 0)
-
-    def drain_d(p, carry):
-        d_over(p).wait_send()
-        d_plane(p).wait_send()
-        d_mate(p, 0).wait_send()
-        d_mate(p, 1).wait_send()
-        return carry
-
-    lax.fori_loop(0, CHUNKS, drain_d, 0)
+    all_of(mate_out, pair_sem.at[0], pair_sem.at[1]).wait_send()
+    shares_done().wait_send()
+
+    for kind, whole in enumerate((gu_whole, d_whole)):
+        all_of(whole, y_send.at[kind], y_send.at[kind]).wait_send()
+        all_of(whole, x_send.at[kind], x_send.at[kind]).wait_send()
+        for second in range(2):
+            all_of(whole, m_send.at[kind, second], m_send.at[kind, second]).wait_send()
 
     def drain(line, carry):
-        for part in range(PIECES):
-            @pl.when((line <= z) & (z < last))
-            def _():
-                tok_copy(line, part, up_send, above).wait_send()
-
-            @pl.when((line >= z) & (z > 0))
-            def _():
-                tok_copy(line, part, down_send, below).wait_send()
+        @pl.when((line <= z) & (z < last))
+        def _():
+            all_of(gath.at[line], up_send.at[line], up_send.at[line]).wait_send()
+
+        @pl.when((line >= z) & (z > 0))
+        def _():
+            all_of(gath.at[line], down_send.at[line], down_send.at[line]).wait_send()
 
         @pl.when(line != z)
         def _():
-            for j in range(CHUNKS):
-                line_copy(0, line, j, above).wait_send()
+            all_of(onward.at[line], line_send.at[line], line_send.at[line]).wait_send()
 
         return carry
 
@@ -717,24 +724,23 @@
             pltpu.VMEM((TP // CORES,) + quarter, bf16),
             pltpu.VMEM(quarter, bf16),
             pltpu.VMEM(quarter, bf16),
-            sem((10,)),
-            sem((2, TP)),
+            sem((9,)),
+            sem((2,)),
+            sem((2,)),
+            sem((2,)),
             sem((lines,)),
             sem((lines,)),
+            sem((lines, PIECES)),
             sem((2,)),
-            sem((lines, PIECES)),
-            sem((lines, PIECES)),
-            sem((lines, PIECES)),
             sem((pieces,)),
+            sem((2,)),
             sem((pieces,)),
-            sem((pieces,)),
-            sem((pieces,)),
-            sem((2, pieces)),
-            sem((2, pieces)),
-            sem((lines, CHUNKS)),
-            sem((2, lines, CHUNKS)),
-            sem((TP // CORES,)),
-            sem((TP // CORES,)),
+            sem((2, 2)),
+            sem((2,)),
+            sem((2, CHUNKS)),
+            sem((lines,)),
+            sem((lines + 1, CHUNKS)),
+            sem((2,)),
             sem,
             sem,
         ],

time: 80 us -> 77.8 us (0.972)
  Pallas kernels: 76.6 us -> 75.1 us
    pallas_call x1, Pallas kernels: 76.6 us -> 75.1 us  [fused_layer(): pl.pallas_call(functools.partial(fused_kernel, lines, width), out_shape=(...]
where the time goes in v3:
time: 77.8 us; the launch traced here: 77.5 us
  Pallas kernels  75.1 us (97%)
  local copies, waits for them, and re-layouts  1.77 us (2%)
    pallas_call x1, Pallas kernels, fused_layer(): pl.pallas_call(functools.partial(fused_kernel, lines, width), out_shape=(...  75.1 us
    unnamed x2, local copies, waits for them, and re-layouts  1.77 us

profile of v3, /device:TPU:17, one launch (start us, length us, event | category | flops | bytes accessed | tf_op | source)
XLA Modules:
  0.0 77.5 jit_solution(17539616951993642561)
XLA Ops:
  0.6 75.1 %shard_map.131 = (bf16[128,2048]{1,0:T(8,128)(2,1)S(1)}, bf16[256,2048]{1,0:T(8,128)(2,1)S(1)}) custom-call(bf16[128,2048]{1,0:T(8,128)(2,1)} %rows_hbm.1, f32[1,2048]{1,0:T(1,128)} %bitcast.13, s32[4,128]{1,0:T(4,128)} %bitcast.14, f32[4,128]{1,0:T(4,128)} %bitcast.15, bf16[2048,512]{1,0:T(8,128)(2,1)} %bitcast.8, bf16[2048,512]{1,0:T(8,128)(2,1)} %bitcast.9, ...), custom_call_target="tpu_custom_call" | custom-call | flops 6442450944 | bytes 16777216 | tf_op jit(solution)/shard_map/pallas_call | solution.py:701
  75.8 1.0 %copy.16 = bf16[256,2048]{1,0:T(8,128)(2,1)} copy(bf16[256,2048]{1,0:T(8,128)(2,1)S(1)} %get-tuple-element.6) | data formatting | bytes 2097152
  76.7 0.8 %copy.17 = bf16[128,2048]{1,0:T(8,128)(2,1)} copy(bf16[128,2048]{1,0:T(8,128)(2,1)S(1)} %get-tuple-element.7) | data formatting | bytes 1048576

commit v4 on v3

--- a/solution.py
+++ b/solution.py
@@ -137,8 +137,8 @@
 PIECES = 4
 CHUNKS = 8
 SLABS = 16
-LAG = 4
-AHEAD = 3
+LAG = 3
+AHEAD = 4
 NORM_ROWS = 16
 
 
@@ -649,9 +649,10 @@
         return carry
 
     keep[x] = keep[x] + mate_in[x].astype(jnp.float32)
-    lax.fori_loop(0, CHUNKS, finish, 0)
+    lax.fori_loop(0, CHUNKS - 1, finish, 0)
     cross_copy().wait_recv()
     attn_ref[...] = (keep[x] + x_in[...].astype(jnp.float32)).astype(jnp.bfloat16)
+    finish(CHUNKS - 1, 0)
 
     @pl.when(ahead)
     def _():

time: 77.8 us -> 76.9 us (0.988); the launches traced: 77.5 us -> 75.7 us
  Pallas kernels: 75.1 us -> 73.3 us
    pallas_call x1, Pallas kernels: 75.1 us -> 73.3 us  [fused_layer(): pl.pallas_call(functools.partial(fused_kernel, lines, width), out_shape=(...]
where the time goes in v4:
time: 76.9 us; the launch traced here: 75.7 us
  Pallas kernels  73.3 us (95%)
  local copies, waits for them, and re-layouts  1.77 us (2%)
    pallas_call x1, Pallas kernels, fused_layer(): pl.pallas_call(functools.partial(fused_kernel, lines, width), out_shape=(...  73.3 us
    unnamed x2, local copies, waits for them, and re-layouts  1.77 us

profile of v4, /device:TPU:17, one launch (start us, length us, event | category | flops | bytes accessed | tf_op | source)
XLA Modules:
  0.0 75.7 jit_solution(3767665693030405576)
XLA Ops:
  0.6 73.3 %shard_map.131 = (bf16[128,2048]{1,0:T(8,128)(2,1)S(1)}, bf16[256,2048]{1,0:T(8,128)(2,1)S(1)}) custom-call(bf16[128,2048]{1,0:T(8,128)(2,1)} %rows_hbm.1, f32[1,2048]{1,0:T(1,128)} %bitcast.13, s32[4,128]{1,0:T(4,128)} %bitcast.14, f32[4,128]{1,0:T(4,128)} %bitcast.15, bf16[2048,512]{1,0:T(8,128)(2,1)} %bitcast.8, bf16[2048,512]{1,0:T(8,128)(2,1)} %bitcast.9, ...), custom_call_target="tpu_custom_call" | custom-call | flops 6442450944 | bytes 16777216 | tf_op jit(solution)/shard_map/pallas_call | solution.py:702
  73.9 1.0 %copy.16 = bf16[256,2048]{1,0:T(8,128)(2,1)} copy(bf16[256,2048]{1,0:T(8,128)(2,1)S(1)} %get-tuple-element.6) | data formatting | bytes 2097152
  74.9 0.8 %copy.17 = bf16[128,2048]{1,0:T(8,128)(2,1)} copy(bf16[128,2048]{1,0:T(8,128)(2,1)S(1)} %get-tuple-element.7) | data formatting | bytes 1048576

commit v5 on v4

--- a/solution.py
+++ b/solution.py
@@ -150,7 +150,7 @@
     raw, gain, routes, route_weight,
     gath, shares, wgu, wd, act, onward, from_line,
     qs, ext, sinks, wo, keep, mate_out, mate_in, x_out, x_in,
-    local_sem, gu_sem, share_sem, halo_sem,
+    local_sem, gu_sem, share_up, share_down, share_recv, halo_sem,
     up_send, down_send, tok_recv,
     y_send, y_recv, x_send, x_recv, m_send, gm_recv, m_recv,
     line_send, line_recv, pair_sem, cross_send, cross_recv,
@@ -223,8 +223,14 @@
     def greet(device):
         pl.semaphore_signal(barrier, inc=1, device_id=device, device_id_type=pl.DeviceIdType.MESH)
 
-    for step in range(1, lines):
-        greet(at(lax.rem(z + step, lines), y, x, c))
+    @pl.when(z < last)
+    def _():
+        greet(above)
+
+    @pl.when(z > 0)
+    def _():
+        greet(below)
+
     greet(over_y)
     greet(over_x)
     greet(mate)
@@ -233,23 +239,22 @@
     def _():
         greet({"ep": skew_ep, "tp": tp})
 
-    pl.semaphore_wait(barrier, last + 3 + jnp.where(skew, 1, 0))
+    beside = jnp.where(z < last, 1, 0) + jnp.where(z > 0, 1, 0)
+    pl.semaphore_wait(barrier, beside + 3 + jnp.where(skew, 1, 0))
 
     halo = remote(
         ext.at[:, pl.ds(attn_rows, WINDOW)], ext.at[:, pl.ds(0, WINDOW)], halo_sem.at[0],
         halo_sem.at[1], {"ep": jnp.minimum(ep + 1, lines * ROW - 1), "tp": tp},
     )
 
-    def share_copy(slot, device):
+    def share_copy(block, upward, device):
+        sems = share_up if upward else share_down
         return remote(
-            shares.at[slot], shares.at[slot], share_sem.at[0], share_sem.at[1], device
+            shares.at[block], shares.at[block], sems.at[block], share_recv.at[block], device
         )
 
     def all_of(view, send, recv):
         return remote(view, view, send, recv, mate)
-
-    def shares_done():
-        return all_of(shares.at[pl.ds(0, last)], share_sem.at[0], share_sem.at[1])
 
     def tok_copy(block, part, sems, device):
         view = gath.at[block, pl.ds(part * piece, piece)]
@@ -322,6 +327,8 @@
     shares[z] = share
 
     def own_tokens(first, count, upward):
+        if first == 0:
+            share_copy(z, upward, above if upward else below).start()
         for part in range(first, first + count):
             if upward:
                 tok_copy(z, part, up_send, above).start()
@@ -346,9 +353,6 @@
     def _():
         own_tokens(half, half, False)
 
-    for step in range(1, lines):
-        other = lax.rem(z + step, lines)
-        share_copy(z, at(other, y, x, c)).start()
     loads[6].wait()
 
     def launch_d(p, carry):
@@ -375,6 +379,14 @@
             @pl.when(i < PIECES * reach)
             def _():
                 tok_copy(block, part, up_send, above).wait_recv()
+
+            @pl.when((i < PIECES * reach) & (part == 0))
+            def _():
+                share_copy(block, upward, above).wait_recv()
+
+            @pl.when((i < PIECES * reach) & (part == 0) & (reach < last))
+            def _():
+                share_copy(block, upward, above if upward else below).start()
 
             @pl.when((i < PIECES * reach) & (reach < last))
             def _():
@@ -503,7 +515,6 @@
         gu_mate(p, 1).start()
         return carry
 
-    shares_done().wait_recv()
     loaded(wgu.at[0, pl.ds(quarter, (TP - 1) * quarter)], gu_sem.at[1])
 
     square = (tok_rows, tok_rows)
@@ -660,7 +671,6 @@
 
     cross_copy().wait_send()
     all_of(mate_out, pair_sem.at[0], pair_sem.at[1]).wait_send()
-    shares_done().wait_send()
 
     for kind, whole in enumerate((gu_whole, d_whole)):
         all_of(whole, y_send.at[kind], y_send.at[kind]).wait_send()
@@ -672,10 +682,12 @@
         @pl.when((line <= z) & (z < last))
         def _():
             all_of(gath.at[line], up_send.at[line], up_send.at[line]).wait_send()
+            share_copy(line, True, above).wait_send()
 
         @pl.when((line >= z) & (z > 0))
         def _():
             all_of(gath.at[line], down_send.at[line], down_send.at[line]).wait_send()
+            share_copy(line, False, below).wait_send()
 
         @pl.when(line != z)
         def _():
@@ -727,7 +739,9 @@
             pltpu.VMEM(quarter, bf16),
             sem((9,)),
             sem((2,)),
-            sem((2,)),
+            sem((lines,)),
+            sem((lines,)),
+            sem((lines,)),
             sem((2,)),
             sem((lines,)),
             sem((lines,)),

time: 76.9 us -> 75.9 us (0.987); the launches traced: 75.7 us -> 75.8 us
  no operation moved by 1% of the time
where the time goes in v5:
time: 75.9 us; the launch traced here: 75.8 us
  Pallas kernels  73.4 us (97%)
  local copies, waits for them, and re-layouts  1.77 us (2%)
    pallas_call x1, Pallas kernels, fused_layer(): pl.pallas_call(functools.partial(fused_kernel, lines, width), out_shape=(...  73.4 us
    unnamed x2, local copies, waits for them, and re-layouts  1.77 us

profile of v5, /device:TPU:17, one launch (start us, length us, event | category | flops | bytes accessed | tf_op | source)
XLA Modules:
  0.0 75.8 jit_solution(10338207271261101523)
XLA Ops:
  0.6 73.4 %shard_map.131 = (bf16[128,2048]{1,0:T(8,128)(2,1)S(1)}, bf16[256,2048]{1,0:T(8,128)(2,1)S(1)}) custom-call(bf16[128,2048]{1,0:T(8,128)(2,1)} %rows_hbm.1, f32[1,2048]{1,0:T(1,128)} %bitcast.13, s32[4,128]{1,0:T(4,128)} %bitcast.14, f32[4,128]{1,0:T(4,128)} %bitcast.15, bf16[2048,512]{1,0:T(8,128)(2,1)} %bitcast.8, bf16[2048,512]{1,0:T(8,128)(2,1)} %bitcast.9, ...), custom_call_target="tpu_custom_call" | custom-call | flops 6442450944 | bytes 16777216 | tf_op jit(solution)/shard_map/pallas_call | solution.py:714
  74.0 1.0 %copy.16 = bf16[256,2048]{1,0:T(8,128)(2,1)} copy(bf16[256,2048]{1,0:T(8,128)(2,1)S(1)} %get-tuple-element.6) | data formatting | bytes 2097152
  75.0 0.8 %copy.17 = bf16[128,2048]{1,0:T(8,128)(2,1)} copy(bf16[128,2048]{1,0:T(8,128)(2,1)S(1)} %get-tuple-element.7) | data formatting | bytes 1048576

commit v6 on v5

--- a/solution.py
+++ b/solution.py
@@ -138,6 +138,7 @@
 CHUNKS = 8
 SLABS = 16
 LAG = 3
+GROUP = 4
 AHEAD = 4
 NORM_ROWS = 16
 
@@ -268,7 +269,7 @@
             pl.ds(expert * hidden + q * (hidden // TP), hidden // TP), pl.ds(p * chunk, chunk)
         ]
 
-    def weight_copies(view, kind, base, mate_recv):
+    def weight_copies(view, kind, base, plane_recv, mate_recv):
         def over_link(p):
             return remote(
                 view(0, tp, p), view(1, tp, p), y_send.at[kind], y_recv.at[base + p], over_y
@@ -276,7 +277,7 @@
 
         def to_plane(p):
             return remote(
-                view(1, tp, p), view(1, tp, p), x_send.at[kind], x_recv.at[base + p], over_x
+                view(1, tp, p), view(1, tp, p), x_send.at[kind], plane_recv(p), over_x
             )
 
         def to_mate(p, second):
@@ -287,9 +288,11 @@
 
         return over_link, to_plane, to_mate
 
-    gu_over, gu_plane, gu_mate = weight_copies(gu_view, 0, 0, lambda second, p: gm_recv.at[second])
+    gu_over, gu_plane, gu_mate = weight_copies(
+        gu_view, 0, 0, lambda p: x_recv.at[p // GROUP], lambda second, p: gm_recv.at[second]
+    )
     d_over, d_plane, d_mate = weight_copies(
-        d_view, 1, SLABS, lambda second, p: m_recv.at[second, p]
+        d_view, 1, SLABS, lambda p: x_recv.at[SLABS // GROUP + p], lambda second, p: m_recv.at[p]
     )
     gu_whole = wgu.at[1, pl.ds(0, quarter)]
     d_whole = wd.at[pl.ds(0, hidden // TP)]
@@ -459,15 +462,20 @@
 
     each = SLABS * WINDOW // attn_rows
 
+    def take_group(g):
+        q = (1 - x) * CORES + c
+        rows = wgu.at[1, pl.ds(q * quarter + g * (GROUP * slab), GROUP * slab)]
+        all_of(rows, x_recv.at[g], x_recv.at[g]).wait_recv()
+        remote(rows, rows, m_send.at[0, 1], gm_recv.at[1], mate).start()
+
     def slot(i, carry):
         gu_over(i).wait_recv()
         gu_plane(i).start()
         gu_mate(i, 0).start()
 
-        @pl.when(i >= LAG)
-        def _():
-            gu_plane(i - LAG).wait_recv()
-            gu_mate(i - LAG, 1).start()
+        @pl.when((i >= LAG + GROUP - 1) & ((i - LAG) % GROUP == GROUP - 1))
+        def _():
+            take_group((i - LAG) // GROUP)
 
         @pl.when(i % each == 0)
         def _():
@@ -510,9 +518,8 @@
         d_plane(j).start()
         d_mate(j, 0).start()
 
-    def late(p, carry):
-        gu_plane(p).wait_recv()
-        gu_mate(p, 1).start()
+    def late(g, carry):
+        take_group(g)
         return carry
 
     loaded(wgu.at[0, pl.ds(quarter, (TP - 1) * quarter)], gu_sem.at[1])
@@ -585,8 +592,8 @@
         def one(j, carry):
             @pl.when(k == 0)
             def _():
-                d_mate(j, 0).wait_recv()
-                d_mate(j, 1).wait_recv()
+                both = wd.at[pl.ds(0, 2 * (hidden // TP)), pl.ds(0, chunk)]
+                all_of(both, m_recv.at[j], m_recv.at[j]).wait_recv()
 
             cols = pl.ds(pl.multiple_of(j * chunk, chunk), chunk)
             own = partial(cols)
@@ -623,7 +630,7 @@
 
     activate(pick(0), 0, 1)
     pass_down(0)
-    lax.fori_loop(SLABS - LAG, SLABS, late, 0)
+    lax.fori_loop((SLABS - LAG) // GROUP, SLABS // GROUP, late, 0)
     for p in range(1, AHEAD - 1):
         pass_down(p)
     for second in range(2):
@@ -749,10 +756,10 @@
             sem((2,)),
             sem((pieces,)),
             sem((2,)),
-            sem((pieces,)),
+            sem((SLABS // GROUP + CHUNKS,)),
             sem((2, 2)),
             sem((2,)),
-            sem((2, CHUNKS)),
+            sem((CHUNKS,)),
             sem((lines,)),
             sem((lines + 1, CHUNKS)),
             sem((2,)),

time: 75.9 us -> 75.7 us (level)
  no operation moved by 1% of the time
where the time goes in v6:
time: 75.7 us; the launch traced here: 75.6 us
  Pallas kernels  73.2 us (97%)
  local copies, waits for them, and re-layouts  1.77 us (2%)
    pallas_call x1, Pallas kernels, fused_layer(): pl.pallas_call(functools.partial(fused_kernel, lines, width), out_shape=(...  73.2 us
    unnamed x2, local copies, waits for them, and re-layouts  1.77 us

profile of v6, /device:TPU:17, one launch (start us, length us, event | category | flops | bytes accessed | tf_op | source)
XLA Modules:
  0.0 75.6 jit_solution(11110785156528571106)
XLA Ops:
  0.6 73.2 %shard_map.131 = (bf16[128,2048]{1,0:T(8,128)(2,1)S(1)}, bf16[256,2048]{1,0:T(8,128)(2,1)S(1)}) custom-call(bf16[128,2048]{1,0:T(8,128)(2,1)} %rows_hbm.1, f32[1,2048]{1,0:T(1,128)} %bitcast.13, s32[4,128]{1,0:T(4,128)} %bitcast.14, f32[4,128]{1,0:T(4,128)} %bitcast.15, bf16[2048,512]{1,0:T(8,128)(2,1)} %bitcast.8, bf16[2048,512]{1,0:T(8,128)(2,1)} %bitcast.9, ...), custom_call_target="tpu_custom_call" | custom-call | flops 6442450944 | bytes 16777216 | tf_op jit(solution)/shard_map/pallas_call | solution.py:721
  73.8 1.0 %copy.16 = bf16[256,2048]{1,0:T(8,128)(2,1)} copy(bf16[256,2048]{1,0:T(8,128)(2,1)S(1)} %get-tuple-element.6) | data formatting | bytes 2097152
  74.8 0.8 %copy.17 = bf16[128,2048]{1,0:T(8,128)(2,1)} copy(bf16[128,2048]{1,0:T(8,128)(2,1)S(1)} %get-tuple-element.7) | data formatting | bytes 1048576
